TPU v7x, 256 devices: a whole 4x4x8 slice. The times are simulated.
256 devices in a mesh: ep: 64 (over z, y, core), tp: 4 (over x).
Axes of the slice: x: 4, y: 4, z: 8, core: 2. Of those that a mesh axis runs over, the one named last changes fastest.
Arguments:
- mix_input: bfloat16 [65536, 2048], P(('ep', 'tp')), may hold values from -6 to 6
- mix_gain: float32 [2048], replicated, may hold values from 0.1 to 1.9
- pool_weight: bfloat16 [4, 512, 512], replicated, may hold values from -0.25 to 0.25
- pool_scale: float32 [2048], replicated, may hold values from 0.1 to 1.9
- moe_input: bfloat16 [32768, 2048], P(('ep', 'tp')), may hold values from -6 to 6
- moe_gain: float32 [2048], replicated, may hold values from 0.1 to 1.9
- expert_ids: int32 [32768, 4], P('ep'), may hold values from 0 to 127, all different within a row; in each aligned block of 128 rows (0 to 127, 128 to 255, ...) at most 6 rows name the same one
- route_score: float32 [32768, 4], P(('ep', 'tp')), may hold values from 0.05 to 1
- expert_gate: bfloat16 [128, 2048, 1024], P('ep', None, 'tp'), may hold values from -0.125 to 0.125
- expert_up: bfloat16 [128, 2048, 1024], P('ep', None, 'tp'), may hold values from -0.125 to 0.125
- expert_down: bfloat16 [128, 1024, 2048], P('ep', 'tp'), may hold values from -0.1875 to 0.1875
- shared_gate: bfloat16 [2048, 512], P(None, 'tp'), may hold values from -0.125 to 0.125
- shared_up: bfloat16 [2048, 512], P(None, 'tp'), may hold values from -0.125 to 0.125
- shared_down: bfloat16 [512, 2048], P('tp'), may hold values from -0.25 to 0.25
Outputs:
- mix_output: bfloat16 [65536, 2048], P(('ep', 'tp'))
- moe_output: bfloat16 [32768, 2048], P(('ep', 'tp'))
Inputs may be any that keep to these rules, and one draw needn't show every extreme that they name: `expert_ids`: each row names 4 different experts. Within each aligned block of 128 rows (the tokens of one device) no expert is named by more than 6 rows, a bound that some block reaches.
All inputs are finite; a program needn't handle non-finite values.
Results may differ from a plain program's by a relative error of at most 0.012.
Values may be sent and summed in bfloat16 or wider, within the bound.
A program may use at most 192 MiB of HBM per device.

v0:
```python
import jax
import jax.numpy as jnp
from jax import lax
from jax.sharding import PartitionSpec as P

WINDOWS = (2, 4, 8, 16)
RMS_EPS = 1e-06
ROUTED_SCALE = 2.5


def passed_along(value, axis, by):
    length = lax.axis_size(axis)
    pairs = [(i, i + by) for i in range(length) if 0 <= i + by < length]
    return lax.ppermute(value, axis, pairs)


def in_one_piece(arrays, axis, dim, along):
    ends, at = ([], 0)
    for a in arrays[:-1]:
        at += a.shape[along]
        ends.append(at)
    both = jnp.concatenate(arrays, axis=along)
    return tuple(jnp.split(lax.all_gather(both, axis, axis=dim, tiled=True), ends, axis=along))


def rms_norm(values, gain_row):
    upcast = values.astype(jnp.float32)
    scaled = upcast * lax.rsqrt(jnp.mean(upcast * upcast, axis=-1, keepdims=True) + RMS_EPS)
    return (scaled * gain_row).astype(jnp.bfloat16)


def rounded(values):
    return lax.optimization_barrier(values.astype(jnp.bfloat16)).astype(jnp.float32)


def window_means(normed, before, offset):
    row_count = normed.shape[0]
    lead_rows = before.shape[0]
    group_size = normed.shape[1] // len(WINDOWS)
    joined = jnp.concatenate([before, normed], axis=0).astype(jnp.float32)
    positions = offset + jnp.arange(row_count, dtype=jnp.int32)
    window_avg = []
    for group_idx, span in enumerate(WINDOWS):
        channels = joined[:, group_idx * group_size : (group_idx + 1) * group_size]
        first_row = lead_rows - span + 1
        running = channels[first_row : first_row + row_count]
        for shift_idx in range(1, span):
            running = running + channels[first_row + shift_idx : first_row + shift_idx + row_count]
        counts = jnp.minimum(positions + 1, span).astype(jnp.float32)
        window_avg.append(running / counts[:, None])
    return jnp.stack(window_avg, axis=1)


def fill_slots(normed, picks, expert_count, capacity):
    tok_count, top_count = picks.shape
    pair_count = tok_count * top_count
    flat_ids = picks.reshape(pair_count)
    matches = flat_ids[:, None] == jnp.arange(expert_count, dtype=jnp.int32)[None, :]
    pair_line = jnp.arange(pair_count, dtype=jnp.int32)
    lower_mask = (pair_line[:, None] > pair_line[None, :]).astype(jnp.bfloat16)
    seen_before = jnp.dot(
        lower_mask, matches.astype(jnp.bfloat16), preferred_element_type=jnp.float32
    )
    rank = jnp.sum(seen_before * matches.astype(jnp.float32), axis=1).astype(jnp.int32)
    slots = flat_ids * capacity + rank
    owner = pair_line // top_count
    slot_token = jnp.full((expert_count * capacity,), tok_count, jnp.int32).at[slots].set(owner)
    padded = jnp.concatenate([normed, jnp.zeros((1, normed.shape[1]), normed.dtype)], axis=0)
    return (padded[slot_token], slots.reshape(tok_count, top_count))


def blockwise_down(hidden, down_rows, pieces, contract):
    block_width = hidden.shape[-1] // pieces
    summed = None
    for part_idx in range(pieces):
        piece_out = jnp.einsum(
            contract,
            hidden[..., part_idx * block_width : (part_idx + 1) * block_width],
            down_rows[..., part_idx * block_width : (part_idx + 1) * block_width, :],
            preferred_element_type=jnp.float32,
        )
        summed = rounded(piece_out) if summed is None else summed + rounded(piece_out)
    return summed.astype(jnp.bfloat16)


def per_device(
    mix_input,
    mix_gain,
    pool_weight,
    pool_scale,
    moe_input,
    moe_gain,
    expert_ids,
    route_score,
    expert_gate,
    expert_up,
    expert_down,
    shared_gate,
    shared_up,
    shared_down,
):
    normed = rms_norm(mix_input, mix_gain)
    row_count, width_all = normed.shape
    reach_rows = max(WINDOWS) - 1
    before = passed_along(normed[row_count - reach_rows :], ("ep", "tp"), 1)
    offset = lax.axis_index(("ep", "tp")) * row_count
    pooled = window_means(normed, before, offset)
    difference = (pooled - normed.astype(jnp.float32).reshape(row_count, len(WINDOWS), -1)).astype(
        jnp.bfloat16
    )
    mixed_out = jnp.einsum(
        "sgc,gcd->sgd", difference, pool_weight, preferred_element_type=jnp.float32
    )
    mix_output = (mixed_out.reshape(row_count, width_all) * pool_scale).astype(jnp.bfloat16)
    h_moe = rms_norm(moe_input, moe_gain)
    tok_count, model_width = h_moe.shape
    top_count = expert_ids.shape[1]
    quarters = lax.axis_size("tp")
    my_quarter = lax.axis_index("tp")
    ep_count = lax.axis_size("ep")
    local_experts = expert_gate.shape[0]
    expert_count = ep_count * local_experts
    capacity = 3 * tok_count * top_count // (2 * expert_count)
    per_source = local_experts * capacity
    full_gate, full_up, full_down, full_sgate, full_sup, full_sdown = (
        *in_one_piece((expert_gate, expert_up), "tp", 2, 0),
        lax.all_gather(expert_down, "tp", axis=1, tiled=True),
        *in_one_piece((shared_gate, shared_up), "tp", 1, 0),
        lax.all_gather(shared_down, "tp", axis=0, tiled=True),
    )
    my_ids = lax.dynamic_slice_in_dim(expert_ids, my_quarter * tok_count, tok_count, 0)
    outgoing, my_slots = fill_slots(h_moe, my_ids, expert_count, capacity)
    landed = lax.all_to_all(
        outgoing.reshape(ep_count, per_source, model_width),
        "ep",
        split_axis=0,
        concat_axis=0,
        tiled=True,
    )
    routed_in = landed.reshape(ep_count, local_experts, capacity, model_width)
    gate_val = jnp.einsum(
        "necd,edf->necf", routed_in, full_gate, preferred_element_type=jnp.float32
    )
    up_val = jnp.einsum("necd,edf->necf", routed_in, full_up, preferred_element_type=jnp.float32)
    hidden = (jax.nn.silu(gate_val) * up_val).astype(jnp.bfloat16)
    expert_back = blockwise_down(hidden, full_down, quarters, "necf,efd->necd")
    expert_back = expert_back.reshape(ep_count, per_source, model_width)
    shared_gate_val = jnp.dot(h_moe, full_sgate, preferred_element_type=jnp.float32)
    shared_up_val = jnp.dot(h_moe, full_sup, preferred_element_type=jnp.float32)
    shared_hidden = (jax.nn.silu(shared_gate_val) * shared_up_val).astype(jnp.bfloat16)
    shared_back = blockwise_down(shared_hidden, full_sdown, quarters, "tf,fd->td")
    returned = lax.all_to_all(expert_back, "ep", split_axis=0, concat_axis=0, tiled=True)
    returned = returned.reshape(expert_count * capacity, model_width)
    route_w = route_score / jnp.sum(route_score, axis=1, keepdims=True) * ROUTED_SCALE
    combined = shared_back.astype(jnp.float32)
    for pick_idx in range(top_count):
        combined = combined + route_w[:, pick_idx : pick_idx + 1] * returned[
            my_slots[:, pick_idx]
        ].astype(jnp.float32)
    return (mix_output, combined.astype(jnp.bfloat16))


def solution(mesh):
    return jax.shard_map(
        per_device,
        mesh=mesh,
        in_specs=(
            P(("ep", "tp"), None),
            P(),
            P(),
            P(),
            P(("ep", "tp"), None),
            P(),
            P("ep", None),
            P(("ep", "tp"), None),
            P("ep", None, "tp"),
            P("ep", None, "tp"),
            P("ep", "tp", None),
            P(None, "tp"),
            P(None, "tp"),
            P("tp", None),
        ),
        out_specs=(P(("ep", "tp"), None), P(("ep", "tp"), None)),
        check_vma=False,
    )
```

profile of v0, /device:TPU:32, one launch (start us, length us, event | category | flops | bytes accessed | tf_op | source)
XLA Modules:
  0.0 439.0 jit_solution(3366335373749575262)
XLA Ops:
  7.2 4.7 %pad_maximum_fusion = bf16[4,2048,256]{2,1,0:T(8,128)(2,1)} fusion(bf16[2,2048,256]{2,1,0:T(8,128)(2,1)} %param.23, bf16[2,2048,256]{2,1,0:T(8,128)(2,1)} %param.22), kind=kLoop, calls=%fused_computation.11 | loop fusion | flops 2097152 | bytes 8388608 | tf_op jit(solution)/shard_map/concatenate | solution.py:22
  14.2 2.4 scatter_custom_fusion
  17.9 4.3 gather_fusion
  22.2 6.1 %reshape.104 = bf16[64,12,2048]{2,1,0:T(8,128)(2,1)} reshape(bf16[768,2048]{1,0:T(8,128)(2,1)} %gather_fusion) | data formatting | bytes 6291456 | tf_op jit(solution)/shard_map/reshape | solution.py:134
  28.4 12.1 %all-to-all-start = ((bf16[64,12,2048]{2,1,0:T(8,128)(2,1)}), bf16[64,12,2048]{2,1,0:T(8,128)(2,1)}, u32[]{:S(2)}, u32[]{:S(2)}) async-start(bf16[64,12,2048]{2,1,0:T(8,128)(2,1)} %reshape.104), calls=%async_computation | async-start | bytes 8388608 | tf_op jit(solution)/shard_map/all_to_all | solution.py:133
  41.8 93.9 %all-to-all-done = bf16[64,12,2048]{2,1,0:T(8,128)(2,1)} async-done(((bf16[64,12,2048]{2,1,0:T(8,128)(2,1)}), bf16[64,12,2048]{2,1,0:T(8,128)(2,1)}, u32[]{:S(2)}, u32[]{:S(2)}) %all-to-all-start) | async-done | bytes 3145760 | tf_op jit(solution)/shard_map/all_to_all | solution.py:133
  135.7 5.6 %copy.28 = bf16[64,12,2048]{2,0,1:T(8,128)(2,1)} copy(bf16[64,12,2048]{2,1,0:T(8,128)(2,1)} %all-to-all-done) | data formatting | bytes 6291456 | tf_op jit(solution)/shard_map/all_to_all | solution.py:133
  141.4 33.7 %all-gather.9.cloned.1.call-done = bf16[4,2048,1024]{2,1,0:T(8,128)(2,1)} async-done(((bf16[4,2048,256]{2,1,0:T(8,128)(2,1)}), bf16[4,2048,1024]{2,1,0:T(8,128)(2,1)}) %all-gather.9.cloned.1.call-update) | async-done | bytes 16777232 | tf_op jit(solution)/shard_map/all_gather | solution.py:23
  175.0 9.3 %fusion = f32[2,1024,64,6]{1,2,3,0:T(8,128)} fusion(bf16[64,2,6,2048]{3,0,2,1:T(8,128)(2,1)} %bitcast.96, bf16[4,2048,1024]{2,1,0:T(8,128)(2,1)} %all-gather.9.cloned.1.call-done), kind=kOutput, calls=%fused_computation.7 | convolution fusion | flops 3221225472 | bytes 14680064 | tf_op jit(solution)/shard_map/necd,edf->necf/dot_general | solution.py:144
  184.3 10.7 %fusion.2 = bf16[64,2,6,1024]{3,0,2,1:T(8,128)(2,1)} fusion(f32[2,1024,64,6]{1,2,3,0:T(8,128)} %fusion, bf16[64,2,6,2048]{3,0,2,1:T(8,128)(2,1)} %bitcast.97, bf16[4,2048,1024]{2,1,0:T(8,128)(2,1)} %all-gather.9.cloned.1.call-done), kind=kOutput, calls=%fused_computation.17 | convolution fusion | flops 3225944064 | bytes 16252928 | tf_op jit(solution)/shard_map/necd,edf->necf/dot_general | solution.py:141
  195.0 67.8 %all-gather.11.cloned.1.call-done = bf16[2,1024,2048]{2,1,0:T(8,128)(2,1)} async-done(((bf16[2,256,2048]{2,1,0:T(8,128)(2,1)}), bf16[2,1024,2048]{2,1,0:T(8,128)(2,1)}) %all-gather.11.cloned.1.call-update) | async-done | bytes 8388624 | tf_op jit(solution)/shard_map/all_gather | solution.py:127
  262.8 2.9 fusion.6
  265.7 3.0 fusion.7
  271.0 3.2 add_convert_fusion
  274.2 3.7 copy.29
  277.9 10.8 %all-to-all-start.1 = ((bf16[64,12,2048]{2,1,0:T(8,128)(2,1)}), bf16[64,12,2048]{2,1,0:T(8,128)(2,1)}, u32[]{:S(2)}, u32[]{:S(2)}) async-start(bf16[64,12,2048]{2,1,0:T(8,128)(2,1)} %copy.29), calls=%async_computation.1 | async-start | bytes 8388608 | tf_op jit(solution)/shard_map/all_to_all | solution.py:152
  289.1 2.9 fusion.62
  292.0 3.6 collective-permute-start
  296.0 86.8 %collective-permute-done = bf16[15,2048]{1,0:T(8,128)(2,1)S(1)} collective-permute-done((bf16[15,2048]{1,0:T(8,128)(2,1)S(1)}, bf16[15,2048]{1,0:T(8,128)(2,1)S(1)}, u32[]{:S(2)}, u32[]{:S(2)}) %collective-permute-start) | collective-permute-done | bytes 61472 | tf_op jit(solution)/shard_map/ppermute | solution.py:14
  387.3 2.9 copy.26
  393.6 2.3 fusion.16
  395.8 2.0 fusion.22
  397.9 2.1 convolution_convert_fusion.7
  400.0 2.1 convolution_convert_fusion.6
  402.2 2.1 convolution_convert_fusion.5
  404.3 2.1 convolution_convert_fusion.4
  406.4 6.2 %reshape.107 = bf16[768,2048]{1,0:T(8,128)(2,1)} reshape(bf16[64,12,2048]{2,1,0:T(8,128)(2,1)} %all-to-all-done.1) | data formatting | bytes 6291456 | tf_op jit(solution)/shard_map/reshape | solution.py:153
  412.6 3.7 gather_fusion.1
  416.3 3.7 gather_fusion.2
  420.1 4.5 %gather_fusion.3 = bf16[128,2048]{1,0:T(8,128)(2,1)} fusion(bf16[768,2048]{1,0:T(8,128)(2,1)} %reshape.107, s32[1024]{0:T(1024)S(1)} %get-tuple-element.26), kind=kCustom, calls=%fused_computation.3 | custom fusion | bytes 1049088 | tf_op jit(solution)/shard_map/gather | solution.py:157
  424.6 4.5 %gather_fusion.4 = bf16[128,2048]{1,0:T(8,128)(2,1)} fusion(bf16[768,2048]{1,0:T(8,128)(2,1)} %reshape.107, s32[1024]{0:T(1024)S(1)} %get-tuple-element.25), kind=kCustom, calls=%fused_computation.4 | custom fusion | bytes 1049088 | tf_op jit(solution)/shard_map/gather | solution.py:157
  429.1 3.4 add_convert_fusion.1
  (75 shorter events, 15.5 us)
Async XLA Ops:
  7.2 377.2 %copy-start = (bf16[4,512,512]{2,1,0:T(8,128)(2,1)S(1)}, bf16[4,512,512]{2,1,0:T(8,128)(2,1)}, u32[]{:S(2)}) copy-start(bf16[4,512,512]{2,1,0:T(8,128)(2,1)} %param.16) | copy-start | bytes 6291460
  7.2 167.8 %all-gather.9.cloned.1.call-start = ((), (), s32[]{:S(2)}) async-start(), calls=%async_computation.4 | async-start | bytes 20971520 | tf_op jit(solution)/shard_map/all_gather | solution.py:23
  11.9 4.7 %copy-start.4 = (bf16[128,2048]{1,0:T(8,128)(2,1)S(1)}, bf16[128,2048]{1,0:T(8,128)(2,1)}, u32[]{:S(2)}) copy-start(bf16[128,2048]{1,0:T(8,128)(2,1)} %param.18) | copy-start | bytes 1572868
  11.9 5.0 %copy-start.10 = (f32[2048]{0:T(1024)S(1)}, f32[2048]{0:T(1024)}, u32[]{:S(2)}) copy-start(f32[2048]{0:T(1024)} %param.19) | copy-start | bytes 24580
  11.9 250.9 %all-gather.11.cloned.1.call-start = ((), (), s32[]{:S(2)}) async-start(), calls=%async_computation.5 | async-start | bytes 10485760 | tf_op jit(solution)/shard_map/all_gather | solution.py:127
  17.0 0.8 copy-start.5
  28.4 12.4 %copy-start.8 = (bf16[2048,128]{1,0:T(8,128)(2,1)S(1)}, bf16[2048,128]{1,0:T(8,128)(2,1)}, u32[]{:S(2)}) copy-start(bf16[2048,128]{1,0:T(8,128)(2,1)} %param.26) | copy-start | bytes 1572868
  28.4 12.4 %copy-start.9 = (bf16[2048,128]{1,0:T(8,128)(2,1)S(1)}, bf16[2048,128]{1,0:T(8,128)(2,1)}, u32[]{:S(2)}) copy-start(bf16[2048,128]{1,0:T(8,128)(2,1)} %param.25) | copy-start | bytes 1572868
  28.4 107.4 %all-to-all-start = ((bf16[64,12,2048]{2,1,0:T(8,128)(2,1)}), bf16[64,12,2048]{2,1,0:T(8,128)(2,1)}, u32[]{:S(2)}, u32[]{:S(2)}) async-start(bf16[64,12,2048]{2,1,0:T(8,128)(2,1)} %reshape.104), calls=%async_computation | async-start | bytes 8388608 | tf_op jit(solution)/shard_map/all_to_all | solution.py:133
  40.5 353.1 %all-gather.5.cloned.1.call-start = ((), (), s32[]{:S(2)}) async-start(), calls=%async_computation.2 | async-start | bytes 5242880 | tf_op jit(solution)/shard_map/all_gather | solution.py:23
  262.8 5.9 %copy-start.2 = (bf16[2,1024,2048]{2,1,0:T(8,128)(2,1)S(1)}, bf16[2,1024,2048]{2,1,0:T(8,128)(2,1)}, u32[]{:S(2)}) copy-start(bf16[2,1024,2048]{2,1,0:T(8,128)(2,1)} %all-gather.11.cloned.1.call-done) | copy-start | bytes 25165828
  265.7 3.0 copy-start.7
  277.9 10.9 %copy-start.3 = (bf16[256,2048]{1,0:T(8,128)(2,1)S(1)}, bf16[256,2048]{1,0:T(8,128)(2,1)}, u32[]{:S(2)}) copy-start(bf16[256,2048]{1,0:T(8,128)(2,1)} %param.14) | copy-start | bytes 3145732
  277.9 11.2 %copy-start.11 = (f32[2048]{0:T(1024)S(1)}, f32[2048]{0:T(1024)}, u32[]{:S(2)}) copy-start(f32[2048]{0:T(1024)} %param.15) | copy-start | bytes 24580
  277.9 128.5 %all-to-all-start.1 = ((bf16[64,12,2048]{2,1,0:T(8,128)(2,1)}), bf16[64,12,2048]{2,1,0:T(8,128)(2,1)}, u32[]{:S(2)}, u32[]{:S(2)}) async-start(bf16[64,12,2048]{2,1,0:T(8,128)(2,1)} %copy.29), calls=%async_computation.1 | async-start | bytes 8388608 | tf_op jit(solution)/shard_map/all_to_all | solution.py:152
  288.8 6.9 %copy-start.13 = (f32[128,4]{0,1:T(4,128)S(1)}, f32[128,4]{0,1:T(4,128)}, u32[]{:S(2)}) copy-start(f32[128,4]{0,1:T(4,128)} %param.21) | copy-start | bytes 6148
  288.8 109.1 %all-gather.7.cloned.1.call-start = ((), (), s32[]{:S(2)}) async-start(), calls=%async_computation.3 | async-start | bytes 2621440 | tf_op jit(solution)/shard_map/all_gather | solution.py:129
  292.0 90.8 %collective-permute-start = (bf16[15,2048]{1,0:T(8,128)(2,1)S(1)}, bf16[15,2048]{1,0:T(8,128)(2,1)S(1)}, u32[]{:S(2)}, u32[]{:S(2)}) collective-permute-start(bf16[15,2048]{1,0:T(8,128)(2,1)S(1)} %slice.264), channel_id=1, source_target_pairs={{0,1},{1,2},{2,3},{3,4},{4,5},{5,6},{6,7},{7,8},{8,9},{9,10},{10,1... | collective-permute-start | bytes 184328 | tf_op jit(solution)/shard_map/ppermute | solution.py:14
  383.7 1.6 copy-start.1
  387.3 2.9 copy-start.12
  393.6 2.3 copy-start.6
Sparse Core Ops, SparseCore 0:
  12.0 162.9 all-gather.8
  176.8 85.9 all-gather.10
  264.6 56.2 all-gather.4
  322.6 33.6 all-gather.6
where the time goes:
time: 440 us; the launch traced here: 439 us
  waiting for transfers between devices  283 us (64%)
  local copies, waits for them, and re-layouts  52.2 us (12%)
  matrix products  43.2 us (10%)
  starting transfers between devices  26.9 us (6%)
  other arithmetic  19.6 us (4%)
  between operations  14.2 us (3%)
    all_to_all x1, waiting for transfers between devices, per_device(): lax.all_to_all(outgoing.reshape(ep_count, per_source, model_width), 'ep',...  93.9 us
    ppermute x1, waiting for transfers between devices, passed_along(): return lax.ppermute(value, axis, pairs)  86.8 us
    all_gather x1, waiting for transfers between devices, per_device(): lax.all_gather(expert_down, 'tp', axis=1, tiled=True)  67.8 us
    all_gather x2, waiting for transfers between devices, in_one_piece(): lax.all_gather(both, axis, axis=dim, tiled=True)  33.7 us
    dot_general x8, matrix products, blockwise_down(): jnp.einsum(contract, hidden[..., part_idx * block_width:(part_idx + 1) *...  16.6 us
    gather x4, local copies, waits for them, and re-layouts, per_device(): returned[my_slots[:, pick_idx]].astype(jnp.float32)  16.5 us
    all_to_all x1, starting transfers between devices, per_device(): lax.all_to_all(outgoing.reshape(ep_count, per_source, model_width), 'ep',...  12.1 us
    all_to_all x1, starting transfers between devices, per_device(): lax.all_to_all(expert_back, 'ep', split_axis=0, concat_axis=0, tiled=True)  10.8 us
  transfers between devices with their start and end apart: 7, of which 4 were waited for; matrix products, arithmetic and copies ran while one was open for 19% of the time, Pallas kernels for 0%

commit v1 on v0

v1 whole, which is shorter than its diff:
```python
import functools

import jax
import jax.numpy as jnp
import numpy as np
from jax import lax
from jax.experimental import pallas as pl
from jax.experimental.pallas import tpu as pltpu
from jax.sharding import PartitionSpec as P

MESH = pl.DeviceIdType.MESH
F32, BF16 = jnp.float32, jnp.bfloat16
WINDOWS = (2, 4, 8, 16)
RMS_EPS = 1e-06
ROUTED_SCALE = 2.5
NZ, NY, NC = 8, 4, 2
COLS = 2
TILE = 256


def rms_norm(values, gain_row):
    upcast = values.astype(F32)
    scaled = upcast * lax.rsqrt(jnp.mean(upcast * upcast, axis=-1, keepdims=True) + RMS_EPS)
    return (scaled * gain_row).astype(BF16)


def dot(a, b):
    return jnp.dot(a, b, preferred_element_type=F32)


def moe_kernel(
    dims,
    x_ref,
    gain_ref,
    meta_ref,
    rep_ref,
    rept_ref,
    tgt_ref,
    tgtt_ref,
    gate_ref,
    up_ref,
    down_ref,
    out_ref,
    hbuf,
    metab,
    pick,
    back,
    wgu,
    wd,
    sendbuf,
    recv,
    xrecv,
    gu,
    psend,
    xback,
    own,
    ret,
    rs_send,
    rs_recv,
    m_sem,
    z_sem,
    ys_sem,
    yr_sem,
    x_sem,
    p_sem,
    r_sem,
    rs_sem,
    wl_sem,
    w_sem,
):
    nz, ny, nx, tok, cap, width = dims
    ring = nz // 2
    peers = ny * NC
    group = nz * cap
    half_rows = peers * group
    rows = 2 * half_rows
    piece = width // COLS
    half = tok // 2
    ep = lax.axis_index("ep")
    tp = lax.axis_index("tp")
    z, q = ep // peers, ep % peers
    y, core = q // NC, q % NC

    def at_z(step):
        return {"ep": ((z + step + nz) % nz) * peers + q}

    def at_peer(dy, dc):
        return {"ep": z * peers + ((y + dy + ny) % ny) * NC + (core + dc + NC) % NC}

    near = tp + 1 - 2 * (tp % 2)
    far = nx - 1 - tp
    weight_side = ({"tp": near}, {"tp": far})
    token_side = ({"tp": far}, {"tp": near})

    barrier = pltpu.get_barrier_semaphore()
    greet = [at_z(1), at_z(-1), {"tp": near}, {"tp": far}]
    greet += [at_peer(r // NC, r % NC) for r in range(1, peers)]
    for device in greet:
        pl.semaphore_signal(barrier, inc=1, device_id=device, device_id_type=MESH)
    pl.semaphore_wait(barrier, len(greet))

    def remote(src, dst, send, recv_, device):
        return pltpu.make_async_remote_copy(
            src_ref=src, dst_ref=dst, send_sem=send, recv_sem=recv_, device_id=device, device_id_type=MESH
        )

    def wait_bytes(ref, sem):
        pltpu.make_async_copy(ref, ref, sem).wait()

    weights = []
    for j in range(2):
        for i, (src, own_dst, far_dst) in enumerate(
            (
                (gate_ref.at[j], wgu.at[j, 0], wgu.at[j, 2]),
                (up_ref.at[j], wgu.at[j, 1], wgu.at[j, 3]),
                (down_ref.at[j], wd.at[j, 0], wd.at[j, 1]),
            )
        ):
            far_copy = remote(src, far_dst, w_sem.at[0, j, i], w_sem.at[1, j, i], weight_side[j])
            own_copy = pltpu.make_async_copy(src, own_dst, wl_sem.at[j, i])
            weights.append((j, far_copy, own_copy))

    hold = rms_norm(x_ref[...], gain_ref[...])
    for g in range(COLS):
        hbuf[g, 0:tok] = hold[:, g * piece : (g + 1) * piece]
    metab[0] = meta_ref[...]

    def meta_copy(d, s):
        src = (-s if d == 0 else s) % nz
        dst = (-s - 1 if d == 0 else s + 1) % nz
        return remote(metab.at[src], metab.at[dst], m_sem.at[0, d, s], m_sem.at[1, d, s], at_z(1 - 2 * d))

    def z_copy(g, d, s, h):
        src = (-s if d == 0 else s) % nz
        dst = (-s - 1 if d == 0 else s + 1) % nz
        return remote(
            hbuf.at[g, pl.ds(src * tok + h * half, half)],
            hbuf.at[g, pl.ds(dst * tok + h * half, half)],
            z_sem.at[0, g, d, s, h],
            z_sem.at[1, g, d, s, h],
            at_z(1 - 2 * d),
        )

    def sends_half(d, s, h):
        return s < ring - 1 or h == d

    def meta_goes(d, s):
        return s < ring - 1 or d == 0

    for d in range(2):
        meta_copy(d, 0).start()
    for h in range(2):
        for d in range(2):
            z_copy(0, d, 0, h).start()
    for j, far_copy, own_copy in weights:
        far_copy.start()
    for j, far_copy, own_copy in weights:
        own_copy.start()

    def z_forward(g, s):
        for h in range(2):
            for d in range(2):
                z_copy(g, d, s - 1, h).wait_recv()
                if sends_half(d, s, h):
                    z_copy(g, d, s, h).start()

    for s in range(1, ring):
        for d in range(2):
            meta_copy(d, s - 1).wait_recv()
            if meta_goes(d, s):
                meta_copy(d, s).start()
    meta_copy(0, ring - 1).wait_recv()

    before = lax.broadcasted_iota(jnp.int32, (tok, tok), 0) < lax.broadcasted_iota(jnp.int32, (tok, tok), 1)
    upper = before.astype(F32).astype(BF16)
    line = lax.broadcasted_iota(jnp.int32, (2 * peers, tok), 0)
    their_core = (core + line % NC) % NC
    their_y = (y + (line % peers) // NC) % ny
    names = (2 * (z * peers + their_y * NC + their_core) + line // peers).astype(F32)

    def tables(zi):
        block = metab[zi].astype(F32)
        named = jnp.zeros((2 * peers, tok), F32)
        weight = jnp.zeros((2 * peers, tok), F32)
        for k in range(4):
            same = (block[k : k + 1] == names).astype(F32)
            named = named + same
            weight = weight + same * block[4 + k : 5 + k]
        rank = dot(named.astype(BF16), upper)
        rank = jnp.where(named > 0.5, rank, -2.0)
        spread = dot(rep_ref[...], rank.astype(BF16))
        pick[:, zi * tok : (zi + 1) * tok] = (spread == tgt_ref[:, zi : zi + 1]).astype(F32).astype(BF16)
        padding = jnp.zeros((tok - 4 * peers, tok), F32)
        turned = jnp.transpose(jnp.concatenate([rank, weight, padding], axis=0))
        spread_t = dot(turned[:, : 2 * peers].astype(BF16), rept_ref[...])
        weight_t = dot(turned[:, 2 * peers : 4 * peers].astype(BF16), rept_ref[...])
        back[zi] = jnp.where(spread_t == tgtt_ref[zi : zi + 1], weight_t, 0.0).astype(BF16)

    for s in range(1, ring):
        z_forward(0, s)
        if s == 1:
            for zi in range(nz):
                tables(zi)
    for g in range(1, COLS):
        for h in range(2):
            for d in range(2):
                z_copy(g, d, 0, h).start()

    def select(g):
        def body(n, _):
            cols = pl.ds(pl.multiple_of(n * TILE, TILE), TILE)
            sendbuf[g, :, cols] = dot(pick[...], hbuf[g, :, cols]).astype(BF16)
            return 0

        lax.fori_loop(0, piece // TILE, body, 0)
        for j in range(2):
            recv[g, j * half_rows : j * half_rows + group] = sendbuf[g, j * half_rows : j * half_rows + group]

    def y_copy(g, j, r):
        part = pl.ds(j * half_rows + r * group, group)
        return remote(
            sendbuf.at[g, part], recv.at[g, part], ys_sem.at[g], yr_sem.at[g, j, r], at_peer(r // NC, r % NC)
        )

    def x_copy(g, j, r):
        part = pl.ds(j * half_rows + r * group, group)
        return remote(recv.at[g, part], xrecv.at[g, part], x_sem.at[0, g, j], x_sem.at[1, g, j], token_side[j])

    order = list(range(1, peers))
    order.sort(key=lambda r: min(r // NC, ny - r // NC))

    def y_start(g):
        for r in order[::-1]:
            for j in range(2):
                y_copy(g, j, r).start()
        for j in range(2):
            x_copy(g, j, 0).start()

    def x_forward(g, some):
        for r in some:
            for j in range(2):
                y_copy(g, j, r).wait_recv()
                x_copy(g, j, r).start()

    def last_z(g):
        for d in range(2):
            z_copy(g, d, ring - 1, d).wait_recv()

    def gate_up(which, g, j):
        src = (recv, xrecv)[which]

        def body(n, _):
            part = dot(src[g, j * half_rows : (j + 1) * half_rows], wgu[j, n, g * piece : (g + 1) * piece])
            if g == 0:
                gu[which, j, n] = part
            else:
                gu[which, j, n] = gu[which, j, n] + part
            return 0

        lax.fori_loop(0, 4, body, 0)

    def hidden(which, j):
        out = []
        for n in (0, 2):
            gate = gu[which, j, n]
            out.append((gate / (1.0 + jnp.exp(-gate)) * gu[which, j, n + 1]).astype(BF16))
        return out

    def down(hid, g, j, dst):
        def body(n, _):
            cols = pl.ds(pl.multiple_of(n * TILE, TILE), TILE)
            wide = pl.ds(pl.multiple_of(g * piece + n * TILE, TILE), TILE)
            dst[g, j, :, cols] = (dot(hid[0], wd[j, 0, :, wide]) + dot(hid[1], wd[j, 1, :, wide])).astype(BF16)
            return 0

        lax.fori_loop(0, piece // TILE, body, 0)

    def p_copy(g, j):
        return remote(psend.at[g, j], xback.at[g, j], p_sem.at[0, g, j], p_sem.at[1, g, j], token_side[j])

    def r_copy(g, j, r):
        return remote(
            own.at[g, j, pl.ds(r * group, group)],
            ret.at[g, pl.ds(j * half_rows + r * group, group)],
            r_sem.at[0, g],
            r_sem.at[1, g],
            at_peer(-(r // NC), -(r % NC)),
        )

    last_z(0)
    select(0)
    y_start(0)
    for s in range(1, ring):
        z_forward(1, s)
        x_forward(0, order[(s - 1) * len(order) // ring : s * len(order) // ring])
    x_forward(0, order[(ring - 1) * len(order) // ring :])
    last_z(1)
    select(1)
    y_start(1)
    for j, far_copy, own_copy in weights:
        own_copy.wait()
        far_copy.wait_recv()
    for j in range(2):
        gate_up(0, 0, j)
    x_forward(1, order)
    for j in range(2):
        wait_bytes(xrecv.at[0, pl.ds(j * half_rows, half_rows)], x_sem.at[1, 0, j])
        gate_up(1, 0, j)
    for j in range(2):
        gate_up(0, 1, j)
    for j in range(2):
        wait_bytes(xrecv.at[1, pl.ds(j * half_rows, half_rows)], x_sem.at[1, 1, j])
        gate_up(1, 1, j)
        hid = hidden(1, j)
        for g in range(COLS):
            down(hid, g, j, psend)
            p_copy(g, j).start()
    for j in range(2):
        hid = hidden(0, j)
        for g in range(COLS):
            down(hid, g, j, own)
    for g in range(COLS):
        for j in range(2):
            p_copy(g, j).wait_recv()
            own[g, j] = (own[g, j].astype(F32) + xback[g, j].astype(F32)).astype(BF16)
            for r in order[::-1]:
                r_copy(g, j, r).start()
            ret[g, j * half_rows : j * half_rows + group] = own[g, j, 0:group]

    def rs_copy(g, d, s):
        part = pl.ds(d * half, half) if s == 0 else pl.ds(0, tok)
        return remote(
            rs_send.at[g, d, s, part],
            rs_recv.at[g, d, s, part],
            rs_sem.at[0, g, d, s],
            rs_sem.at[1, g, d, s],
            at_z(1 - 2 * d),
        )

    def share(g, zi, first, count, adds, dst, dst_at):
        def body(n, _):
            cols = pl.ds(pl.multiple_of(n * TILE, TILE), TILE)
            total = dot(back[zi, first : first + count], ret[g, :, cols])
            for d, s in adds:
                total = total + rs_recv[g, d, s, first : first + count, cols].astype(F32)
            place = pl.ds(pl.multiple_of(dst_at + n * TILE, TILE), TILE)
            if dst is None:
                out_ref[first : first + count, place] = total
            else:
                dst[first : first + count, place] = total.astype(BF16)
            return 0

        lax.fori_loop(0, piece // TILE, body, 0)

    def rs_step(g, s):
        for d in range(2):
            zi = ring - s if d == 0 else ring + s
            dst = rs_send.at[g, d, s]
            if s > 0:
                rs_copy(g, d, s - 1).wait_recv()
            if s == 0:
                share(g, zi, d * half, half, (), dst, 0)
            elif s == 1:
                for h in range(2):
                    share(g, zi, h * half, half, ((d, 0),) if h == d else (), dst, 0)
            else:
                share(g, zi, 0, tok, ((d, s - 1),), dst, 0)
            rs_copy(g, d, s).start()

    def rs_last(g):
        for d in range(2):
            rs_copy(g, d, ring - 1).wait_recv()
        share(g, 0, 0, tok, ((0, ring - 1), (1, ring - 1)), None, g * piece)

    def ret_wait(g):
        far_rows = 2 * (half_rows - group)
        wait_bytes(ret.at[g, pl.ds(0, far_rows)], r_sem.at[1, g])

    ret_wait(0)
    for s in range(ring):
        rs_step(0, s)
        if s == 0:
            ret_wait(1)
        else:
            rs_step(1, s - 1)
    rs_step(1, ring - 1)
    rs_last(0)
    rs_last(1)

    for d in range(2):
        for s in range(ring):
            if meta_goes(d, s):
                meta_copy(d, s).wait_send()
    for g in range(COLS):
        for d in range(2):
            for s in range(ring):
                for h in range(2):
                    if sends_half(d, s, h):
                        z_copy(g, d, s, h).wait_send()
                rs_copy(g, d, s).wait_send()
        far_rows = 2 * (half_rows - group)
        wait_bytes(sendbuf.at[g, pl.ds(0, far_rows)], ys_sem.at[g])
        wait_bytes(ret.at[g, pl.ds(0, far_rows)], r_sem.at[0, g])
        for j in range(2):
            wait_bytes(recv.at[g, pl.ds(0, half_rows)], x_sem.at[0, g, j])
            p_copy(g, j).wait_send()
    for j, far_copy, own_copy in weights:
        far_copy.wait_send()


def routed(dims, moe_input, gain, meta, gate, up, down):
    nz, ny, nx, tok, cap, width = dims
    peers, ring = ny * NC, nz // 2
    group = nz * cap
    half_rows = peers * group
    rows = 2 * half_rows
    piece = width // COLS
    hid = gate.shape[2]
    line = np.arange(rows)
    rep = (line[:, None] // group == np.arange(2 * peers)[None, :]).astype(np.float32)
    turn = (line // cap) % nz
    tgt = np.where(turn[:, None] == np.arange(nz)[None, :], (line % cap)[:, None], -1).astype(np.float32)
    vmem = pl.BlockSpec(memory_space=pltpu.VMEM)
    hbm = pl.BlockSpec(memory_space=pl.ANY)
    dma = pltpu.SemaphoreType.DMA
    return pl.pallas_call(
        functools.partial(moe_kernel, dims),
        out_shape=jax.ShapeDtypeStruct((tok, width), F32),
        in_specs=[vmem] * 7 + [hbm] * 3,
        out_specs=vmem,
        scratch_shapes=[
            pltpu.VMEM((COLS, nz * tok, piece), BF16),
            pltpu.VMEM((nz, 16, tok), BF16),
            pltpu.VMEM((rows, nz * tok), BF16),
            pltpu.VMEM((nz, tok, rows), BF16),
            pltpu.VMEM((2, 4, width, hid), BF16),
            pltpu.VMEM((2, 2, hid, width), BF16),
            pltpu.VMEM((COLS, rows, piece), BF16),
            pltpu.VMEM((COLS, rows, piece), BF16),
            pltpu.VMEM((COLS, rows, piece), BF16),
            pltpu.VMEM((2, 2, 4, half_rows, hid), F32),
            pltpu.VMEM((COLS, 2, half_rows, piece), BF16),
            pltpu.VMEM((COLS, 2, half_rows, piece), BF16),
            pltpu.VMEM((COLS, 2, half_rows, piece), BF16),
            pltpu.VMEM((COLS, rows, piece), BF16),
            pltpu.VMEM((COLS, 2, ring, tok, piece), BF16),
            pltpu.VMEM((COLS, 2, ring, tok, piece), BF16),
            dma((2, 2, ring)),
            dma((2, COLS, 2, ring, 2)),
            dma((COLS,)),
            dma((COLS, 2, peers)),
            dma((2, COLS, 2)),
            dma((2, COLS, 2)),
            dma((2, COLS)),
            dma((2, COLS, 2, ring)),
            dma((2, 3)),
            dma((2, 2, 3)),
        ],
        compiler_params=pltpu.CompilerParams(
            collective_id=0, has_side_effects=True, vmem_limit_bytes=67043328
        ),
        cost_estimate=pl.CostEstimate(flops=40 * 10**9, bytes_accessed=200 * 10**6, transcendentals=0),
    )(
        moe_input,
        gain.reshape(1, width),
        meta,
        jnp.asarray(rep, BF16),
        jnp.asarray(rep.T, BF16),
        jnp.asarray(tgt),
        jnp.asarray(tgt.T),
        gate,
        up,
        down,
    )


def passed_along(value, axis, by):
    length = lax.axis_size(axis)
    pairs = [(i, i + by) for i in range(length) if 0 <= i + by < length]
    return lax.ppermute(value, axis, pairs)


def window_means(normed, before, offset):
    row_count = normed.shape[0]
    lead_rows = before.shape[0]
    group_size = normed.shape[1] // len(WINDOWS)
    joined = jnp.concatenate([before, normed], axis=0).astype(F32)
    positions = offset + jnp.arange(row_count, dtype=jnp.int32)
    window_avg = []
    for group_idx, span in enumerate(WINDOWS):
        channels = joined[:, group_idx * group_size : (group_idx + 1) * group_size]
        first_row = lead_rows - span + 1
        running = channels[first_row : first_row + row_count]
        for shift_idx in range(1, span):
            running = running + channels[first_row + shift_idx : first_row + shift_idx + row_count]
        counts = jnp.minimum(positions + 1, span).astype(F32)
        window_avg.append(running / counts[:, None])
    return jnp.stack(window_avg, axis=1)


def in_one_piece(arrays, axis, dim, along):
    ends, at = ([], 0)
    for a in arrays[:-1]:
        at += a.shape[along]
        ends.append(at)
    both = jnp.concatenate(arrays, axis=along)
    return tuple(jnp.split(lax.all_gather(both, axis, axis=dim, tiled=True), ends, axis=along))


def per_device(
    sizes,
    mix_input,
    mix_gain,
    pool_weight,
    pool_scale,
    moe_input,
    moe_gain,
    expert_ids,
    route_score,
    expert_gate,
    expert_up,
    expert_down,
    shared_gate,
    shared_up,
    shared_down,
):
    nz, ny = sizes
    nx = lax.axis_size("tp")
    tok, width = moe_input.shape
    experts = lax.axis_size("ep") * expert_gate.shape[0]
    cap = 3 * tok * expert_ids.shape[1] // (2 * experts)
    my_ids = lax.dynamic_slice_in_dim(expert_ids, lax.axis_index("tp") * tok, tok, 0)
    route_w = route_score / jnp.sum(route_score, axis=1, keepdims=True) * ROUTED_SCALE
    meta = jnp.concatenate(
        [my_ids.T.astype(BF16), route_w.T.astype(BF16), jnp.zeros((8, tok), BF16)], axis=0
    )
    dims = (nz, ny, nx, tok, cap, width)
    routed_out = routed(dims, moe_input, moe_gain, meta, expert_gate, expert_up, expert_down)

    h_moe = rms_norm(moe_input, moe_gain)
    full_sgate, full_sup = in_one_piece((shared_gate, shared_up), "tp", 1, 0)
    full_sdown = lax.all_gather(shared_down, "tp", axis=0, tiled=True)
    shared_gate_val = dot(h_moe, full_sgate)
    shared_up_val = dot(h_moe, full_sup)
    shared_hidden = (jax.nn.silu(shared_gate_val) * shared_up_val).astype(BF16)
    shared_back = dot(shared_hidden, full_sdown)
    moe_output = (routed_out + shared_back).astype(BF16)

    normed = rms_norm(mix_input, mix_gain)
    row_count, width_all = normed.shape
    reach_rows = max(WINDOWS) - 1
    before = passed_along(normed[row_count - reach_rows :], ("ep", "tp"), 1)
    offset = lax.axis_index(("ep", "tp")) * row_count
    pooled = window_means(normed, before, offset)
    difference = (pooled - normed.astype(F32).reshape(row_count, len(WINDOWS), -1)).astype(BF16)
    mixed_out = jnp.einsum("sgc,gcd->sgd", difference, pool_weight, preferred_element_type=F32)
    mix_output = (mixed_out.reshape(row_count, width_all) * pool_scale).astype(BF16)
    return (mix_output, moe_output)


def solution(mesh, sizes=(NZ, NY)):
    return jax.shard_map(
        functools.partial(per_device, sizes),
        mesh=mesh,
        in_specs=(
            P(("ep", "tp"), None),
            P(),
            P(),
            P(),
            P(("ep", "tp"), None),
            P(),
            P("ep", None),
            P(("ep", "tp"), None),
            P("ep", None, "tp"),
            P("ep", None, "tp"),
            P("ep", "tp", None),
            P(None, "tp"),
            P(None, "tp"),
            P("tp", None),
        ),
        out_specs=(P(("ep", "tp"), None), P(("ep", "tp"), None)),
        check_vma=False,
    )
```

time: 440 us -> 308 us (0.70)
  waiting for transfers between devices: 283 us -> 0.06 us
  Pallas kernels: 0 us -> 265 us
  local copies, waits for them, and re-layouts: 52.2 us -> 6.59 us
  matrix products: 43.2 us -> 8.15 us
  starting transfers between devices: 26.9 us -> 3.47 us
  other arithmetic: 19.6 us -> 10.1 us
    pallas_call x0 -> x1, Pallas kernels: none -> 265 us  [routed(): pl.pallas_call(functools.partial(moe_kernel, dims), out_shape=jax.ShapeDt...]
    all_to_all x2 -> x0, waiting for transfers between devices: 93.9 us -> none  [the longest x1 93.9 us: per_device(): lax.all_to_all(outgoing.reshape(ep_count, per_source, model_width), 'ep',...]
    ppermute x1, waiting for transfers between devices: 86.8 us -> 0.01 us  [passed_along(): return lax.ppermute(value, axis, pairs)]
    all_gather x2 -> x1, waiting for transfers between devices: 67.8 us -> 0.02 us  [per_device(): full_sdown = lax.all_gather(shared_down, 'tp', axis=0, tiled=True)]
    dot_general x13 -> x2, matrix products: 41.2 us -> 6.08 us  [dot(): return jnp.dot(a, b, preferred_element_type=F32)]
    all_gather x2 -> x1, waiting for transfers between devices: 33.7 us -> 0.01 us  [in_one_piece(): lax.all_gather(both, axis, axis=dim, tiled=True)]
    all_to_all x2 -> x0, starting transfers between devices: 22.9 us -> none  [the longest x1 12.1 us: per_device(): lax.all_to_all(outgoing.reshape(ep_count, per_source, model_width), 'ep',...]
    gather x5 -> x0, local copies, waits for them, and re-layouts: 20.9 us -> none  [the longest x4 16.5 us: per_device(): returned[my_slots[:, pick_idx]].astype(jnp.float32)]
  transfers between devices with their start and end apart: 7 -> 3, of which waited for: 4 -> 0; matrix products, arithmetic and copies ran while one was open for 19% -> 5% of each run, Pallas kernels for 0% -> 86%
where the time goes in v1:
time: 308 us; the launch traced here: 307 us
  Pallas kernels  265 us (86%)
  between operations  14.2 us (5%)
  other arithmetic  10.1 us (3%)
  matrix products  8.15 us (3%)
  local copies, waits for them, and re-layouts  6.59 us (2%)
  starting transfers between devices  3.47 us (1%)
    pallas_call x1, Pallas kernels, routed(): pl.pallas_call(functools.partial(moe_kernel, dims), out_shape=jax.ShapeDt...  265 us
  transfers between devices with their start and end apart: 3, of which 0 were waited for; matrix products, arithmetic and copies ran while one was open for 5% of the time, Pallas kernels for 86%

profile of v1, /device:TPU:32, one launch (start us, length us, event | category | flops | bytes accessed | tf_op | source)
XLA Modules:
  0.0 307.4 jit_solution(11131003786290281594)
XLA Ops:
  7.2 0.0 all-gather.3.cloned.1.call-start
  7.2 2.4 pad_maximum_fusion
  9.6 0.0 all-gather.3.cloned.1.call-update
  9.7 0.0 all-gather.5.cloned.1.call-start
  9.7 0.3 fusion.1
  10.0 0.0 copy-start.7
  10.0 1.6 fusion.43
  11.7 1.0 copy-done.1
  12.7 0.6 slice.158
  13.3 3.4 %collective-permute-start = (bf16[15,2048]{1,0:T(8,128)(2,1)}, bf16[15,2048]{1,0:T(8,128)(2,1)}, u32[]{:S(2)}, u32[]{:S(2)}) collective-permute-start(bf16[15,2048]{1,0:T(8,128)(2,1)} %slice.158), channel_id=1, source_target_pairs={{0,1},{1,2},{2,3},{3,4},{4,5},{5,6},{6,7},{7,8},{8,9},{9,10},{10,1... | collective-permute-start | bytes 184328 | tf_op jit(solution)/shard_map/ppermute | solution.py:480
  16.7 0.0 all-gather.5.cloned.1.call-update
  16.8 0.7 fusion.39
  17.5 0.1 pad.4.clone
  17.5 0.7 maximum_maximum_fusion.meta_ref
  18.2 264.8 %shard_map.185 = f32[128,2048]{1,0:T(8,128)} custom-call(bf16[128,2048]{1,0:T(8,128)(2,1)} %x_ref.1, f32[1,2048]{1,0:T(1,128)} %bitcast.28, bf16[16,128]{1,0:T(8,128)(2,1)} %maximum_maximum_fusion.meta_ref, bf16[768,16]{1,0:T(8,128)(2,1)} %constant.53.clone.rep_ref, bf16[16,768]{1,0:T(8,128)(2,1)} %constant.54.clone.rept_ref, ...), custom_call_target="tpu_custom_call" | custom-call | flops 40000000000 | bytes 200000000 | tf_op jit(solution)/shard_map/pallas_call | solution.py:426
  283.0 1.2 fusion.18
  284.3 0.0 collective-permute-done
  284.3 1.5 maximum_convert_fusion
  285.8 0.5 fusion.23
  286.4 0.0 copy-start.3
  286.4 0.7 fusion.29
  287.1 0.9 copy-done
  288.0 0.6 copy-done.3
  288.6 2.1 convolution_bitcast_fusion
  290.7 1.9 copy.22
  292.6 0.0 copy-start.8
  292.7 0.3 fusion.9
  293.0 0.0 copy-start.4
  293.0 1.4 copy.23
  294.4 2.2 fusion.7
  296.6 0.0 all-gather.5.cloned.1.call-done
  296.7 3.9 %fusion = bf16[128,2048]{1,0:T(8,128)(2,1)} fusion(f32[128,2048]{1,0:T(8,128)S(1)} %copy-done.9, bf16[512,2048]{1,0:T(8,128)(2,1)} %all-gather.5.cloned.1.call-done, bf16[4096,512]{1,0:T(8,128)(2,1)} %all-gather.3.cloned.1.call-done, f32[128,512]{1,0:T(8,128)S(1)} %fusion.7, bf16[128,2048]{1,0:T(8,128)(2,1)S(1)} %copy-done.4, f32[2048]{0:T(1024)S(1)} %copy-done.8, ...), kind=kOutput, calls=%fused_computation.3 | convolution fusion | flops 538836992 | bytes 6562304 | tf_op jit(solution)/shard_map/dot_general | solution.py:28
  (21 shorter events, 0.1 us)
Async XLA Ops:
  7.2 2.5 copy-start.2
  7.2 2.8 copy-start.5
  7.2 287.3 %all-gather.3.cloned.1.call-start = ((), (), s32[]{:S(2)}) async-start(), calls=%async_computation | async-start | bytes 5242880 | tf_op jit(solution)/shard_map/all_gather | solution.py:507
  9.7 287.0 %all-gather.5.cloned.1.call-start = ((), (), s32[]{:S(2)}) async-start(), calls=%async_computation.1 | async-start | bytes 2621440 | tf_op jit(solution)/shard_map/all_gather | solution.py:542
  10.0 6.7 %copy-start.7 = (f32[128,4]{0,1:T(4,128)S(1)}, f32[128,4]{0,1:T(4,128)}, u32[]{:S(2)}) copy-start(f32[128,4]{0,1:T(4,128)} %param.25) | copy-start | bytes 6148
  11.7 1.0 copy-start.1
  13.3 271.0 %collective-permute-start = (bf16[15,2048]{1,0:T(8,128)(2,1)}, bf16[15,2048]{1,0:T(8,128)(2,1)}, u32[]{:S(2)}, u32[]{:S(2)}) collective-permute-start(bf16[15,2048]{1,0:T(8,128)(2,1)} %slice.158), channel_id=1, source_target_pairs={{0,1},{1,2},{2,3},{3,4},{4,5},{5,6},{6,7},{7,8},{8,9},{9,10},{10,1... | collective-permute-start | bytes 184328 | tf_op jit(solution)/shard_map/ppermute | solution.py:480
  286.4 1.6 copy-start
  286.4 2.2 copy-start.3
  290.7 1.9 copy-start.6
  292.6 1.8 copy-start.8
  293.0 1.4 copy-start.4
  294.4 2.2 copy-start.9
Sparse Core Ops, SparseCore 0:
  9.8 91.9 all-gather.2
  103.6 51.2 all-gather.4

commit v2 on v1

v2 whole, which is shorter than its diff:
```python
import functools

import jax
import jax.numpy as jnp
import numpy as np
from jax import lax
from jax.experimental import pallas as pl
from jax.experimental.pallas import tpu as pltpu
from jax.sharding import PartitionSpec as P

MESH = pl.DeviceIdType.MESH
F32, BF16 = jnp.float32, jnp.bfloat16
WINDOWS = (2, 4, 8, 16)
RMS_EPS = 1e-06
ROUTED_SCALE = 2.5
NZ, NY, NC = 8, 4, 2
COLS = 2
PARTS = 4
TILE = 256


def rms_norm(values, gain_row):
    upcast = values.astype(F32)
    scaled = upcast * lax.rsqrt(jnp.mean(upcast * upcast, axis=-1, keepdims=True) + RMS_EPS)
    return (scaled * gain_row).astype(BF16)


def dot(a, b):
    return jnp.dot(a, b, preferred_element_type=F32)


def fused_kernel(
    dims,
    x_ref,
    gain_ref,
    ids_ref,
    score_ref,
    rep_ref,
    rept_ref,
    tgt_ref,
    tgtt_ref,
    mix_gain_ref,
    scale_ref,
    mix_ref,
    pool_ref,
    gate_ref,
    up_ref,
    down_ref,
    sgate_ref,
    sup_ref,
    sdown_ref,
    mix_out,
    moe_out,
    hbuf,
    metab,
    pick,
    back,
    wgu,
    wd,
    sendbuf,
    recv,
    xrecv,
    gu,
    hidb,
    xback,
    ret,
    rs_recv,
    shared,
    sg,
    su,
    sd,
    mixb,
    halo,
    pool,
    diff,
    mixed,
    m_sem,
    z_sem,
    ys_sem,
    yr_sem,
    x_sem,
    p_sem,
    r_sem,
    rs_sem,
    wl_sem,
    w_sem,
    wd_sem,
    sx_sem,
    sy_sem,
    sz_sem,
    sc_sem,
    mix_sem,
    halo_sem,
):
    nz, ny, nx, tok, cap, width = dims
    ring = nz // 2
    peers = ny * NC
    group = nz * cap
    half_rows = peers * group
    piece = width // COLS
    part_width = width // PARTS
    per_col = PARTS // COLS
    half = tok // 2
    ep = lax.axis_index("ep")
    tp = lax.axis_index("tp")
    z, q = ep // peers, ep % peers
    y, core = q // NC, q % NC

    def at_z(step):
        return {"ep": ((z + step + nz) % nz) * peers + q}

    def peer_of(dy, dc):
        return ((y + dy + ny) % ny) * NC + (core + dc + NC) % NC

    def at_peer(dy, dc):
        return {"ep": z * peers + peer_of(dy, dc)}

    def at_line(step):
        count = lax.axis_size("ep") * nx
        line = (ep * nx + tp + step + count) % count
        return {"ep": line // nx, "tp": line % nx}

    near = tp + 1 - 2 * (tp % 2)
    far = nx - 1 - tp
    weight_side = ({"tp": near}, {"tp": far})
    token_side = ({"tp": far}, {"tp": near})

    barrier = pltpu.get_barrier_semaphore()
    greet = [at_z(1), at_z(-1), {"tp": near}, {"tp": far}, {"tp": (tp + 2) % nx}, at_line(1), at_line(-1)]
    greet += [at_peer(r // NC, r % NC) for r in range(1, peers)]
    for device in greet:
        pl.semaphore_signal(barrier, inc=1, device_id=device, device_id_type=MESH)
    with jax.named_scope("barrier"):
        pl.semaphore_wait(barrier, len(greet))

    def remote(src, dst, send, recv_, device):
        return pltpu.make_async_remote_copy(
            src_ref=src, dst_ref=dst, send_sem=send, recv_sem=recv_, device_id=device, device_id_type=MESH
        )

    def wait_bytes(ref, sem):
        pltpu.make_async_copy(ref, ref, sem).wait()

    def wide_copies(j):
        return [
            remote(src.at[j], wgu.at[j, 2 + i], w_sem.at[0, j, i], w_sem.at[1, j, i], weight_side[j])
            for i, src in enumerate((gate_ref, up_ref))
        ]

    def down_copy(j, p):
        cols = pl.ds(p * part_width, part_width)
        return remote(
            down_ref.at[j, :, cols], wd.at[j, 1, :, cols], wd_sem.at[0, j, p], wd_sem.at[1, j, p], weight_side[j]
        )

    def own_copies(j):
        return [
            pltpu.make_async_copy(gate_ref.at[j], wgu.at[j, 0], wl_sem.at[j, 0]),
            pltpu.make_async_copy(up_ref.at[j], wgu.at[j, 1], wl_sem.at[j, 1]),
            pltpu.make_async_copy(down_ref.at[j], wd.at[j, 0], wl_sem.at[j, 2]),
        ]

    for j in range(2):
        for copy in wide_copies(j):
            copy.start()

    hold = rms_norm(x_ref[...], gain_ref[...])
    for g in range(COLS):
        hbuf[g, 0:tok] = hold[:, g * piece : (g + 1) * piece]

    def meta_copy(d, s):
        src = (-s if d == 0 else s) % nz
        dst = (-s - 1 if d == 0 else s + 1) % nz
        return remote(metab.at[src], metab.at[dst], m_sem.at[0, d, s], m_sem.at[1, d, s], at_z(1 - 2 * d))

    def z_copy(g, d, s, h):
        src = (-s if d == 0 else s) % nz
        dst = (-s - 1 if d == 0 else s + 1) % nz
        return remote(
            hbuf.at[g, pl.ds(src * tok + h * half, half)],
            hbuf.at[g, pl.ds(dst * tok + h * half, half)],
            z_sem.at[0, g, d, s, h],
            z_sem.at[1, g, d, s, h],
            at_z(1 - 2 * d),
        )

    def sends_half(d, s, h):
        return s < ring - 1 or h == d

    def meta_goes(d, s):
        return s < ring - 1 or d == 0

    def z_first(g):
        for h in range(2):
            for d in range(2):
                z_copy(g, d, 0, h).start()

    def z_forward(g, s):
        for h in range(2):
            for d in range(2):
                z_copy(g, d, s - 1, h).wait_recv()
                if sends_half(d, s, h):
                    z_copy(g, d, s, h).start()

    def last_z(g):
        for d in range(2):
            z_copy(g, d, ring - 1, d).wait_recv()

    z_first(0)
    my_ids = ids_ref[pl.ds(pl.multiple_of(tp * tok, tok), tok)].astype(F32)
    scores = score_ref[...]
    route = scores / jnp.sum(scores, axis=1, keepdims=True) * ROUTED_SCALE
    tagged = jnp.concatenate([my_ids, route, jnp.zeros((tok, tok - 8), F32)], axis=1)
    metab[0] = jnp.transpose(tagged)[:16].astype(BF16)
    for d in range(2):
        meta_copy(d, 0).start()

    for j in range(2):
        for copy in own_copies(j):
            copy.start()
    pieces = ((sgate_ref, sg, sg.shape[1] // peers), (sup_ref, su, su.shape[1] // peers), (sdown_ref, sd, sd.shape[1] // peers))
    shared_own = [pltpu.make_async_copy(src, dst.at[0], sc_sem.at[0, a]) for a, (src, dst, _) in enumerate(pieces)]
    mix_copies = [
        pltpu.make_async_copy(mix_ref, mixb, mix_sem.at[0]),
        pltpu.make_async_copy(pool_ref, pool, mix_sem.at[1]),
    ]
    reach = halo.shape[0]
    halo_copy = remote(
        mix_ref.at[pl.ds(mix_ref.shape[0] - reach, reach)], halo, halo_sem.at[0], halo_sem.at[1], at_line(1)
    )
    for copy in shared_own + mix_copies + [halo_copy]:
        copy.start()

    def piece_at(dst, size, which):
        return dst.at[pl.ds(1, nx - 1), pl.ds(which * size, size)]

    def shared_x(a, step):
        src, dst, size = pieces[a]
        rows_at = pl.ds(q * size, size)
        return remote(
            src.at[rows_at], dst.at[nx - step, rows_at], sx_sem.at[0, a], sx_sem.at[1, a], {"tp": (tp + step) % nx}
        )

    def shared_x_wait(a, side):
        _, dst, size = pieces[a]
        wait_bytes(dst.at[pl.ds(1, nx - 1), pl.ds(0, size)], sx_sem.at[side, a])

    def shared_y(a, d):
        _, dst, size = pieces[a]
        ref = piece_at(dst, size, q)
        return remote(ref, ref, sy_sem.at[0, a, d], sy_sem.at[1, a, d], at_peer(1 - 2 * d, 0))

    def shared_y2(a):
        d = a % 2
        _, dst, size = pieces[a]
        ref = piece_at(dst, size, peer_of(2 * d - 1, 0))
        return remote(ref, ref, sz_sem.at[0, a], sz_sem.at[1, a], at_peer(1 - 2 * d, 0))

    def shared_core(a, dy):
        _, dst, size = pieces[a]
        ref = piece_at(dst, size, peer_of(dy, 0))
        return remote(ref, ref, sc_sem.at[1, a], sc_sem.at[2, a], at_peer(0, 1))

    def shared_core_wait(a, side):
        _, dst, size = pieces[a]
        wait_bytes(dst.at[pl.ds(1, nx - 1), pl.ds(0, ny * size)], sc_sem.at[1 + side, a])

    for a in range(3):
        for step in (1, nx - 1, 2):
            shared_x(a, step).start()

    before = lax.broadcasted_iota(jnp.int32, (tok, tok), 0) < lax.broadcasted_iota(jnp.int32, (tok, tok), 1)
    upper = before.astype(F32).astype(BF16)
    line = lax.broadcasted_iota(jnp.int32, (2 * peers, tok), 0)
    their_core = (core + line % NC) % NC
    their_y = (y + (line % peers) // NC) % ny
    names = (2 * (z * peers + their_y * NC + their_core) + line // peers).astype(F32)

    def tables(zi):
        block = metab[zi].astype(F32)
        named = jnp.zeros((2 * peers, tok), F32)
        weight = jnp.zeros((2 * peers, tok), F32)
        for k in range(4):
            same = (block[k : k + 1] == names).astype(F32)
            named = named + same
            weight = weight + same * block[4 + k : 5 + k]
        rank = dot(named.astype(BF16), upper)
        rank = jnp.where(named > 0.5, rank, -2.0)
        spread = dot(rep_ref[...], rank.astype(BF16))
        pick[:, zi * tok : (zi + 1) * tok] = (spread == tgt_ref[:, zi : zi + 1]).astype(F32).astype(BF16)
        padding = jnp.zeros((tok - 4 * peers, tok), F32)
        turned = jnp.transpose(jnp.concatenate([rank, weight, padding], axis=0))
        spread_t = dot(turned[:, : 2 * peers].astype(BF16), rept_ref[...])
        weight_t = dot(turned[:, 2 * peers : 4 * peers].astype(BF16), rept_ref[...])
        back[zi] = jnp.where(spread_t == tgtt_ref[zi : zi + 1], weight_t, 0.0).astype(BF16)

    def select(g):
        def body(n, _):
            cols = pl.ds(pl.multiple_of(n * TILE, TILE), TILE)
            sendbuf[g, :, cols] = dot(pick[...], hbuf[g, :, cols]).astype(BF16)
            return 0

        lax.fori_loop(0, piece // TILE, body, 0)
        for j in range(2):
            recv[g, j * half_rows : j * half_rows + group] = sendbuf[g, j * half_rows : j * half_rows + group]

    def y_copy(g, j, r):
        part = pl.ds(j * half_rows + r * group, group)
        return remote(
            sendbuf.at[g, part], recv.at[g, part], ys_sem.at[g], yr_sem.at[g, j, r], at_peer(r // NC, r % NC)
        )

    def x_copy(g, j, r):
        part = pl.ds(j * half_rows + r * group, group)
        return remote(recv.at[g, part], xrecv.at[g, part], x_sem.at[0, g, j], x_sem.at[1, g, j], token_side[j])

    order = list(range(1, peers))
    order.sort(key=lambda r: min(r // NC, ny - r // NC))

    def y_start(g):
        for r in order[::-1]:
            for j in range(2):
                y_copy(g, j, r).start()
        for j in range(2):
            x_copy(g, j, 0).start()

    def x_forward(g, some):
        for r in some:
            for j in range(2):
                y_copy(g, j, r).wait_recv()
                x_copy(g, j, r).start()

    def gate_up(which, g, j):
        src = (recv, xrecv)[which]

        def body(n, _):
            part = dot(src[g, j * half_rows : (j + 1) * half_rows], wgu[j, n, g * piece : (g + 1) * piece])
            if g == 0:
                gu[which, j, n] = part
            else:
                gu[which, j, n] = gu[which, j, n] + part
            return 0

        lax.fori_loop(0, 4, body, 0)

    def hidden(which, j):
        for i in range(2):
            gate = gu[which, j, i * 2]
            hidb[which, j, i] = (gate / (1.0 + jnp.exp(-gate)) * gu[which, j, i * 2 + 1]).astype(BF16)

    def down(which, p, j, dst):
        g = p // per_col

        def body(n, _):
            cols = pl.ds(pl.multiple_of((p % per_col) * part_width + n * TILE, TILE), TILE)
            wide = pl.ds(pl.multiple_of(p * part_width + n * TILE, TILE), TILE)
            val = dot(hidb[which, j, 0], wd[j, 0, :, wide]) + dot(hidb[which, j, 1], wd[j, 1, :, wide])
            dst[g, j * half_rows : (j + 1) * half_rows, cols] = val.astype(BF16)
            return 0

        lax.fori_loop(0, part_width // TILE, body, 0)

    def at_part(ref, p, rows_at):
        return ref.at[p // per_col, rows_at, pl.ds((p % per_col) * part_width, part_width)]

    def p_copy(p, j):
        rows_at = pl.ds(j * half_rows, half_rows)
        return remote(
            at_part(sendbuf, p, rows_at), at_part(xback, p, rows_at), p_sem.at[0, p, j], p_sem.at[1, p, j], token_side[j]
        )

    def r_copy(p, j, r):
        rows_at = pl.ds(j * half_rows + r * group, group)
        return remote(
            at_part(recv, p, rows_at),
            at_part(ret, p, rows_at),
            r_sem.at[0, p],
            r_sem.at[1, p],
            at_peer(-(r // NC), -(r % NC)),
        )

    def mixer():
        for copy in mix_copies:
            copy.wait()
        halo_copy.wait_recv()
        count = mixb.shape[0]
        lead = jnp.where(ep * nx + tp > 0, 1.0, 0.0)
        body_in = mixb[...].astype(F32)
        halo_in = halo[...].astype(F32) * lead
        scales = [
            lax.rsqrt(jnp.mean(v * v, axis=-1, keepdims=True) + RMS_EPS) for v in (halo_in, body_in)
        ]
        position = (ep * nx + tp) * count + lax.broadcasted_iota(jnp.int32, (count, 1), 0)
        span_width = width // len(WINDOWS)
        for g, span in enumerate(WINDOWS):
            counts = jnp.minimum(position + 1, span).astype(F32)
            for n in range(span_width // TILE):
                cols = slice(g * span_width + n * TILE, g * span_width + (n + 1) * TILE)
                gain = mix_gain_ref[:, cols]
                top = (halo[:, cols].astype(F32) * lead * scales[0] * gain).astype(BF16).astype(F32)
                rest = (mixb[:, cols].astype(F32) * scales[1] * gain).astype(BF16).astype(F32)
                total = jnp.concatenate([top, rest], axis=0)
                step = 1
                while step < span:
                    total = total + pltpu.roll(total, step, 0)
                    step *= 2
                diff[:, n * TILE : (n + 1) * TILE] = (total[reach:] / counts - rest).astype(BF16)
            cols = slice(g * span_width, (g + 1) * span_width)
            mixed[:, cols] = (dot(diff[...], pool[g]) * scale_ref[:, cols]).astype(BF16)
        pltpu.make_async_copy(mixed, mix_out, mix_sem.at[2]).start()

    def shared_expert():
        for a in range(3):
            shared_own[a].wait()
            shared_core_wait(a, 1)
        again = rms_norm(x_ref[...], gain_ref[...])
        tokens = [again[:, g * piece : (g + 1) * piece] for g in range(COLS)]
        hids = []
        for i in range(nx):
            gate = dot(tokens[0], sg[i, :piece]) + dot(tokens[1], sg[i, piece:])
            up = dot(tokens[0], su[i, :piece]) + dot(tokens[1], su[i, piece:])
            hids.append((gate / (1.0 + jnp.exp(-gate)) * up).astype(BF16))

        def body(n, _):
            cols = pl.ds(pl.multiple_of(n * TILE, TILE), TILE)
            total = dot(hids[0], sd[0, :, cols])
            for i in range(1, nx):
                total = total + dot(hids[i], sd[i, :, cols])
            shared[:, cols] = total
            return 0

        lax.fori_loop(0, width // TILE, body, 0)

    def rs_at(ref, p, d, s, first, count):
        return ref.at[
            p // per_col,
            pl.ds((d * ring + s) * tok + first, count),
            pl.ds((p % per_col) * part_width, part_width),
        ]

    def rs_copy(p, d, s):
        first, count = (d * half, half) if s == 0 else (0, tok)
        return remote(
            rs_at(hbuf, p, d, s, first, count),
            rs_at(rs_recv, p, d, s, first, count),
            rs_sem.at[0, p, d, s],
            rs_sem.at[1, p, d, s],
            at_z(1 - 2 * d),
        )

    def share(p, zi, first, count, adds, place):
        g = p // per_col

        def body(n, _):
            cols = pl.ds(pl.multiple_of((p % per_col) * part_width + n * TILE, TILE), TILE)
            total = dot(back[zi, first : first + count], ret[g, :, cols])
            for d, s in adds:
                at = (d * ring + s) * tok + first
                total = total + rs_recv[g, at : at + count, cols].astype(F32)
            if place is None:
                wide = pl.ds(pl.multiple_of(p * part_width + n * TILE, TILE), TILE)
                moe_out[first : first + count, wide] = (total + shared[first : first + count, wide]).astype(BF16)
            else:
                hbuf[g, place + first : place + first + count, cols] = total.astype(BF16)
            return 0

        lax.fori_loop(0, part_width // TILE, body, 0)

    def rs_step(p, s):
        for d in range(2):
            zi = ring - s if d == 0 else ring + s
            place = (d * ring + s) * tok
            if s > 0:
                with jax.named_scope(f"rswait{p}_{s}"):
                    rs_copy(p, d, s - 1).wait_recv()
            if s == 0:
                share(p, zi, d * half, half, (), place)
            elif s == 1:
                for h in range(2):
                    share(p, zi, h * half, half, ((d, 0),) if h == d else (), place)
            else:
                share(p, zi, 0, tok, ((d, s - 1),), place)
            rs_copy(p, d, s).start()

    def rs_last(p):
        with jax.named_scope(f"rswait{p}_last"):
            for d in range(2):
                rs_copy(p, d, ring - 1).wait_recv()
        share(p, 0, 0, tok, ((0, ring - 1), (1, ring - 1)), None)

    def ret_wait(p):
        with jax.named_scope(f"retwait{p}"):
            far_rows = 2 * (half_rows - group)
            wait_bytes(at_part(ret, p, pl.ds(0, far_rows)), r_sem.at[1, p])

    def give_back(p):
        cols = slice((p % per_col) * part_width, (p % per_col + 1) * part_width)
        g = p // per_col
        for j in range(2):
            with jax.named_scope(f"pwait{p}{j}"):
                p_copy(p, j).wait_recv()
            span = slice(j * half_rows, (j + 1) * half_rows)
            recv[g, span, cols] = (recv[g, span, cols].astype(F32) + xback[g, span, cols].astype(F32)).astype(BF16)
            for r in order[::-1]:
                r_copy(p, j, r).start()
            first = slice(j * half_rows, j * half_rows + group)
            ret[g, first, cols] = recv[g, first, cols]

    for s in range(1, ring):
        with jax.named_scope(f"z0_{s}"):
            for d in range(2):
                meta_copy(d, s - 1).wait_recv()
                if meta_goes(d, s):
                    meta_copy(d, s).start()
            z_forward(0, s)
    z_first(1)
    meta_copy(0, ring - 1).wait_recv()
    with jax.named_scope("tables"):
        for zi in range(nz):
            tables(zi)
    with jax.named_scope("last_z0"):
        last_z(0)
    with jax.named_scope("select0"):
        select(0)
        y_start(0)
    for s in range(1, ring):
        with jax.named_scope(f"z1_{s}"):
            z_forward(1, s)
        with jax.named_scope(f"xfwd0_{s}"):
            x_forward(0, order[(s - 1) * len(order) // ring : s * len(order) // ring])
        for j in range(2):
            down_copy(j, s - 1).start()
    with jax.named_scope("xfwd0_rest"):
        x_forward(0, order[(ring - 1) * len(order) // ring :])
    with jax.named_scope("last_z1"):
        last_z(1)
    with jax.named_scope("select1"):
        select(1)
        y_start(1)
    for j in range(2):
        for p in range(ring - 1, PARTS):
            down_copy(j, p).start()
    with jax.named_scope("weights"):
        for j in range(2):
            for copy in own_copies(j):
                copy.wait()
            for copy in wide_copies(j):
                copy.wait_recv()
    with jax.named_scope("own_gu0"):
        for j in range(2):
            gate_up(0, 0, j)
    with jax.named_scope("xfwd1"):
        x_forward(1, order)
    with jax.named_scope("shared_x"):
        for a in range(3):
            shared_x_wait(a, 1)
            for d in range(2):
                shared_y(a, d).start()
    with jax.named_scope("mixer"):
        mixer()
    with jax.named_scope("shared_y"):
        for a in range(3):
            for d in range(2):
                shared_y(a, d).wait_recv()
            shared_y2(a).start()
            for dy in (0, 1, -1):
                shared_core(a, dy).start()
    for j in range(2):
        with jax.named_scope(f"xwait0_{j}"):
            wait_bytes(xrecv.at[0, pl.ds(j * half_rows, half_rows)], x_sem.at[1, 0, j])
        with jax.named_scope("par_gu0"):
            gate_up(1, 0, j)
    with jax.named_scope("own_gu1"):
        for j in range(2):
            gate_up(0, 1, j)
            hidden(0, j)
    far_rows = 2 * (half_rows - group)
    for g in range(COLS):
        wait_bytes(sendbuf.at[g, pl.ds(0, far_rows)], ys_sem.at[g])
    for j in range(2):
        with jax.named_scope(f"xwait1_{j}"):
            wait_bytes(xrecv.at[1, pl.ds(j * half_rows, half_rows)], x_sem.at[1, 1, j])
        with jax.named_scope("par_gu1"):
            gate_up(1, 1, j)
            hidden(1, j)
    for p in range(PARTS):
        for j in range(2):
            with jax.named_scope(f"wd{p}{j}"):
                down_copy(j, p).wait_recv()
            with jax.named_scope("par_down"):
                down(1, p, j, sendbuf)
                p_copy(p, j).start()
    for g in range(COLS):
        for j in range(2):
            wait_bytes(recv.at[g, pl.ds(0, half_rows)], x_sem.at[0, g, j])
    with jax.named_scope("own_down"):
        for p in range(PARTS):
            for j in range(2):
                down(0, p, j, recv)
    for g in range(COLS):
        for d in range(2):
            for s in range(ring):
                for h in range(2):
                    if sends_half(d, s, h):
                        z_copy(g, d, s, h).wait_send()
    with jax.named_scope("shared"):
        for a in range(3):
            shared_y2(a).wait_recv()
            shared_core(a, 2).start()
        shared_expert()

    events = []
    for p in range(PARTS):
        events.append((9 * p, give_back, (p,)))
        events.append((9 * p + 11, ret_wait, (p,)))
        for s in range(ring):
            events.append((9 * p + 12 + 5 * s, rs_step, (p, s)))
        events.append((9 * p + 12 + 5 * ring, rs_last, (p,)))
    for _, act, args in sorted(events, key=lambda e: e[0]):
        act(*args)

    pltpu.make_async_copy(mixed, mix_out, mix_sem.at[2]).wait()
    halo_copy.wait_send()
    for d in range(2):
        for s in range(ring):
            if meta_goes(d, s):
                meta_copy(d, s).wait_send()
    for p in range(PARTS):
        wait_bytes(at_part(ret, p, pl.ds(0, far_rows)), r_sem.at[0, p])
        for d in range(2):
            for s in range(ring):
                rs_copy(p, d, s).wait_send()
        for j in range(2):
            p_copy(p, j).wait_send()
            down_copy(j, p).wait_send()
    for j in range(2):
        for copy in wide_copies(j):
            copy.wait_send()
    for a in range(3):
        shared_x_wait(a, 0)
        shared_y2(a).wait_send()
        shared_core_wait(a, 0)
        for d in range(2):
            shared_y(a, d).wait_send()


def fused(dims, moe_input, moe_gain, ids, scores, mix_gain, scale, mix_input, pool, routed, shared):
    nz, ny, nx, tok, cap, width = dims
    peers, ring = ny * NC, nz // 2
    group = nz * cap
    half_rows = peers * group
    rows = 2 * half_rows
    piece = width // COLS
    hid = routed[0].shape[2]
    sh = shared[0].shape[1]
    count = mix_input.shape[0]
    line = np.arange(rows)
    rep = (line[:, None] // group == np.arange(2 * peers)[None, :]).astype(np.float32)
    turn = (line // cap) % nz
    tgt = np.where(turn[:, None] == np.arange(nz)[None, :], (line % cap)[:, None], -1).astype(np.float32)
    vmem = pl.BlockSpec(memory_space=pltpu.VMEM)
    hbm = pl.BlockSpec(memory_space=pl.ANY)
    dma = pltpu.SemaphoreType.DMA
    return pl.pallas_call(
        functools.partial(fused_kernel, dims),
        out_shape=(jax.ShapeDtypeStruct((count, width), BF16), jax.ShapeDtypeStruct((tok, width), BF16)),
        in_specs=[vmem] * 10 + [hbm] * 8,
        out_specs=(hbm, vmem),
        scratch_shapes=[
            pltpu.VMEM((COLS, nz * tok, piece), BF16),
            pltpu.VMEM((nz, 16, tok), BF16),
            pltpu.VMEM((rows, nz * tok), BF16),
            pltpu.VMEM((nz, tok, rows), BF16),
            pltpu.VMEM((2, 4, width, hid), BF16),
            pltpu.VMEM((2, 2, hid, width), BF16),
            pltpu.VMEM((COLS, rows, piece), BF16),
            pltpu.VMEM((COLS, rows, piece), BF16),
            pltpu.VMEM((COLS, rows, piece), BF16),
            pltpu.VMEM((2, 2, 4, half_rows, hid), F32),
            pltpu.VMEM((2, 2, 2, half_rows, hid), BF16),
            pltpu.VMEM((COLS, rows, piece), BF16),
            pltpu.VMEM((COLS, rows, piece), BF16),
            pltpu.VMEM((COLS, nz * tok, piece), BF16),
            pltpu.VMEM((tok, width), F32),
            pltpu.VMEM((nx, width, sh), BF16),
            pltpu.VMEM((nx, width, sh), BF16),
            pltpu.VMEM((nx, sh, width), BF16),
            pltpu.VMEM((count, width), BF16),
            pltpu.VMEM((16, width), BF16),
            pltpu.VMEM(pool.shape, BF16),
            pltpu.VMEM((count, width // len(WINDOWS)), BF16),
            pltpu.VMEM((count, width), BF16),
            dma((2, 2, ring)),
            dma((2, COLS, 2, ring, 2)),
            dma((COLS,)),
            dma((COLS, 2, peers)),
            dma((2, COLS, 2)),
            dma((2, PARTS, 2)),
            dma((2, PARTS)),
            dma((2, PARTS, 2, ring)),
            dma((2, 3)),
            dma((2, 2, 2)),
            dma((2, 2, PARTS)),
            dma((2, 3)),
            dma((2, 3, 2)),
            dma((2, 3)),
            dma((3, 3)),
            dma((3,)),
            dma((2,)),
        ],
        compiler_params=pltpu.CompilerParams(
            collective_id=0, has_side_effects=True, vmem_limit_bytes=67043328
        ),
    )(
        moe_input,
        moe_gain.reshape(1, width),
        ids,
        scores,
        jnp.asarray(rep, BF16),
        jnp.asarray(rep.T, BF16),
        jnp.asarray(tgt),
        jnp.asarray(tgt.T),
        mix_gain.reshape(1, width),
        scale.reshape(1, width),
        mix_input,
        pool,
        *routed,
        *shared,
    )


def per_device(
    sizes,
    mix_input,
    mix_gain,
    pool_weight,
    pool_scale,
    moe_input,
    moe_gain,
    expert_ids,
    route_score,
    expert_gate,
    expert_up,
    expert_down,
    shared_gate,
    shared_up,
    shared_down,
):
    nz, ny = sizes
    tok, width = moe_input.shape
    experts = lax.axis_size("ep") * expert_gate.shape[0]
    cap = 3 * tok * expert_ids.shape[1] // (2 * experts)
    dims = (nz, ny, lax.axis_size("tp"), tok, cap, width)
    return fused(
        dims,
        moe_input,
        moe_gain,
        expert_ids,
        route_score,
        mix_gain,
        pool_scale,
        mix_input,
        pool_weight,
        (expert_gate, expert_up, expert_down),
        (shared_gate, shared_up, shared_down),
    )


def solution(mesh, sizes=(NZ, NY)):
    return jax.shard_map(
        functools.partial(per_device, sizes),
        mesh=mesh,
        in_specs=(
            P(("ep", "tp"), None),
            P(),
            P(),
            P(),
            P(("ep", "tp"), None),
            P(),
            P("ep", None),
            P(("ep", "tp"), None),
            P("ep", None, "tp"),
            P("ep", None, "tp"),
            P("ep", "tp", None),
            P(None, "tp"),
            P(None, "tp"),
            P("tp", None),
        ),
        out_specs=(P(("ep", "tp"), None), P(("ep", "tp"), None)),
        check_vma=False,
    )
```

time: 308 us -> 213 us (0.69)
  Pallas kernels: 265 us -> 204 us
  between operations: 14.2 us -> 0.65 us
  other arithmetic: 10.1 us -> 0 us
  matrix products: 8.15 us -> 0 us
  starting transfers between devices: 3.47 us -> 0 us
    pallas_call x1, Pallas kernels: 265 us -> 204 us  [fused(): pl.pallas_call(functools.partial(fused_kernel, dims), out_shape=(jax.Shap...]
    dot_general x3 -> x0, matrix products: 8.15 us -> none  [the longest x2 6.08 us: dot(): return jnp.dot(a, b, preferred_element_type=F32)]
    ppermute x1 -> x0, starting transfers between devices: 3.39 us -> none  [passed_along(): return lax.ppermute(value, axis, pairs)]
  transfers between devices with their start and end apart: 3 -> 0, of which waited for: 0 -> 0; matrix products, arithmetic and copies ran while one was open for 5% -> 0% of each run, Pallas kernels for 86% -> 0%
where the time goes in v2:
time: 213 us; the launch traced here: 211 us
  Pallas kernels  204 us (96%)
  local copies, waits for them, and re-layouts  6.12 us (3%)
    pallas_call x1, Pallas kernels, fused(): pl.pallas_call(functools.partial(fused_kernel, dims), out_shape=(jax.Shap...  204 us
    unnamed x6, local copies, waits for them, and re-layouts  6.12 us

profile of v2, /device:TPU:32, one launch (start us, length us, event | category | flops | bytes accessed | tf_op | source)
XLA Modules:
  0.0 210.9 jit_solution(10452705985232732604)
XLA Ops:
  0.6 1.4 copy.21.score_ref
  2.0 1.5 copy.20.ids_ref
  3.6 204.1 %shard_map.185 = (bf16[256,2048]{1,0:T(8,128)(2,1)}, bf16[128,2048]{1,0:T(8,128)(2,1)}) custom-call(bf16[128,2048]{1,0:T(8,128)(2,1)} %x_ref.1, f32[1,2048]{1,0:T(1,128)} %bitcast.3, s32[512,4]{1,0:T(8,128)} %copy.20.ids_ref, f32[128,4]{1,0:T(8,128)} %copy.21.score_ref, bf16[768,16]{1,0:T(8,128)(2,1)} %constant.8.clone.rep_ref, ...), custom_call_target="tpu_custom_call" | custom-call | tf_op jit(solution)/shard_map/pallas_call | solution.py:664
  207.7 0.0 copy-start
  207.7 2.4 %copy.24 = bf16[256,2048]{1,0:T(8,128)(2,1)} copy(bf16[256,2048]{1,0:T(8,128)(2,1)} %get-tuple-element.4) | data formatting | bytes 2097152
  210.1 0.0 copy-done
  210.1 0.8 copy.25
Async XLA Ops:
  207.7 2.4 %copy-start = (bf16[128,2048]{1,0:T(8,128)(2,1)S(1)}, bf16[128,2048]{1,0:T(8,128)(2,1)}, u32[]{:S(2)}) copy-start(bf16[128,2048]{1,0:T(8,128)(2,1)} %get-tuple-element.5) | copy-start | bytes 1572868

commit v3 on v2

--- a/solution.py
+++ b/solution.py
@@ -15,8 +15,11 @@
 ROUTED_SCALE = 2.5
 NZ, NY, NC = 8, 4, 2
 COLS = 2
-PARTS = 4
+WIDTHS = (256, 256, 256, 256, 256, 256, 256, 128, 128)
+PARTS = len(WIDTHS)
 TILE = 256
+GAP, HOP, LEAD, GIVE, AHEAD = 7.0, 5.5, 3.0, 1.0, 2
+SHARED_AT = (6.5, 16.2, 27.5)
 
 
 def rms_norm(values, gain_row):
@@ -31,14 +34,14 @@
 
 def fused_kernel(
     dims,
-    x_ref,
+    x_hbm,
     gain_ref,
     ids_ref,
     score_ref,
-    rep_ref,
-    rept_ref,
-    tgt_ref,
-    tgtt_ref,
+    rep_hbm,
+    rept_hbm,
+    tgt_hbm,
+    tgtt_hbm,
     mix_gain_ref,
     scale_ref,
     mix_ref,
@@ -62,6 +65,7 @@
     xrecv,
     gu,
     hidb,
+    own,
     xback,
     ret,
     rs_recv,
@@ -72,6 +76,11 @@
     mixb,
     halo,
     pool,
+    x_ref,
+    rep_ref,
+    rept_ref,
+    tgt_ref,
+    tgtt_ref,
     diff,
     mixed,
     m_sem,
@@ -88,9 +97,11 @@
     sx_sem,
     sy_sem,
     sz_sem,
+    sr_sem,
     sc_sem,
     mix_sem,
     halo_sem,
+    in_sem,
 ):
     nz, ny, nx, tok, cap, width = dims
     ring = nz // 2
@@ -98,8 +109,18 @@
     group = nz * cap
     half_rows = peers * group
     piece = width // COLS
-    part_width = width // PARTS
-    per_col = PARTS // COLS
+    scale = width // sum(WIDTHS)
+    starts = [sum(WIDTHS[:p]) * scale for p in range(PARTS)]
+    widths = [w * scale for w in WIDTHS]
+
+    def col_of(p):
+        return starts[p] // piece
+
+    def cols_of(p):
+        return slice(starts[p] % piece, starts[p] % piece + widths[p])
+
+    def span_of(p):
+        return pl.ds(starts[p] % piece, widths[p])
     half = tok // 2
     ep = lax.axis_index("ep")
     tp = lax.axis_index("tp")
@@ -125,8 +146,17 @@
     weight_side = ({"tp": near}, {"tp": far})
     token_side = ({"tp": far}, {"tp": near})
 
+    loads = [
+        pltpu.make_async_copy(src, dst, in_sem.at[i])
+        for i, (src, dst) in enumerate(
+            ((x_hbm, x_ref), (rep_hbm, rep_ref), (rept_hbm, rept_ref), (tgt_hbm, tgt_ref), (tgtt_hbm, tgtt_ref))
+        )
+    ]
+    for copy in loads:
+        copy.start()
+
     barrier = pltpu.get_barrier_semaphore()
-    greet = [at_z(1), at_z(-1), {"tp": near}, {"tp": far}, {"tp": (tp + 2) % nx}, at_line(1), at_line(-1)]
+    greet = [at_z(step) for step in range(1, nz)] + [{"tp": near}, {"tp": far}, {"tp": (tp + 2) % nx}, at_line(1), at_line(-1)]
     greet += [at_peer(r // NC, r % NC) for r in range(1, peers)]
     for device in greet:
         pl.semaphore_signal(barrier, inc=1, device_id=device, device_id_type=MESH)
@@ -148,7 +178,7 @@
         ]
 
     def down_copy(j, p):
-        cols = pl.ds(p * part_width, part_width)
+        cols = pl.ds(starts[p], widths[p])
         return remote(
             down_ref.at[j, :, cols], wd.at[j, 1, :, cols], wd_sem.at[0, j, p], wd_sem.at[1, j, p], weight_side[j]
         )
@@ -164,6 +194,7 @@
         for copy in wide_copies(j):
             copy.start()
 
+    loads[0].wait()
     hold = rms_norm(x_ref[...], gain_ref[...])
     for g in range(COLS):
         hbuf[g, 0:tok] = hold[:, g * piece : (g + 1) * piece]
@@ -207,11 +238,10 @@
             z_copy(g, d, ring - 1, d).wait_recv()
 
     z_first(0)
-    my_ids = ids_ref[pl.ds(pl.multiple_of(tp * tok, tok), tok)].astype(F32)
+    my_ids = ids_ref[:, pl.ds(pl.multiple_of(tp * tok, tok), tok)].astype(F32)
     scores = score_ref[...]
-    route = scores / jnp.sum(scores, axis=1, keepdims=True) * ROUTED_SCALE
-    tagged = jnp.concatenate([my_ids, route, jnp.zeros((tok, tok - 8), F32)], axis=1)
-    metab[0] = jnp.transpose(tagged)[:16].astype(BF16)
+    route = scores / jnp.sum(scores, axis=0, keepdims=True) * ROUTED_SCALE
+    metab[0] = jnp.concatenate([my_ids, route, jnp.zeros((8, tok), F32)], axis=0).astype(BF16)
     for d in range(2):
         meta_copy(d, 0).start()
 
@@ -234,16 +264,37 @@
     def piece_at(dst, size, which):
         return dst.at[pl.ds(1, nx - 1), pl.ds(which * size, size)]
 
+    def crumb(a):
+        _, dst, size = pieces[a]
+        if a < 2:
+            small = size // nz
+            return (pl.ds(q * size + z * small, small),)
+        small = dst.shape[2] // nz
+        return (pl.ds(q * size, size), pl.ds(pl.multiple_of(z * small, small), small))
+
+    def crumbs(a, count):
+        _, dst, size = pieces[a]
+        if a < 2:
+            return dst.at[pl.ds(1, nx - 1), pl.ds(0, count * (size // nz))]
+        return dst.at[pl.ds(1, nx - 1), pl.ds(0, size), pl.ds(0, count * (dst.shape[2] // nz))]
+
     def shared_x(a, step):
-        src, dst, size = pieces[a]
-        rows_at = pl.ds(q * size, size)
+        src, dst, _ = pieces[a]
+        at = crumb(a)
         return remote(
-            src.at[rows_at], dst.at[nx - step, rows_at], sx_sem.at[0, a], sx_sem.at[1, a], {"tp": (tp + step) % nx}
+            src.at[at], dst.at[(nx - step, *at)], sx_sem.at[0, a], sx_sem.at[1, a], {"tp": (tp + step) % nx}
         )
 
     def shared_x_wait(a, side):
-        _, dst, size = pieces[a]
-        wait_bytes(dst.at[pl.ds(1, nx - 1), pl.ds(0, size)], sx_sem.at[side, a])
+        wait_bytes(crumbs(a, 1), sx_sem.at[side, a])
+
+    def shared_z(a, step):
+        _, dst, _ = pieces[a]
+        ref = dst.at[(pl.ds(1, nx - 1), *crumb(a))]
+        return remote(ref, ref, sr_sem.at[0, a], sr_sem.at[1, a], at_z(step))
+
+    def shared_z_wait(a, side):
+        wait_bytes(crumbs(a, nz - 1), sr_sem.at[side, a])
 
     def shared_y(a, d):
         _, dst, size = pieces[a]
@@ -292,7 +343,7 @@
         turned = jnp.transpose(jnp.concatenate([rank, weight, padding], axis=0))
         spread_t = dot(turned[:, : 2 * peers].astype(BF16), rept_ref[...])
         weight_t = dot(turned[:, 2 * peers : 4 * peers].astype(BF16), rept_ref[...])
-        back[zi] = jnp.where(spread_t == tgtt_ref[zi : zi + 1], weight_t, 0.0).astype(BF16)
+        back[zi * tok : (zi + 1) * tok] = jnp.where(spread_t == tgtt_ref[zi : zi + 1], weight_t, 0.0).astype(BF16)
 
     def select(g):
         def body(n, _):
@@ -335,49 +386,54 @@
 
         def body(n, _):
             part = dot(src[g, j * half_rows : (j + 1) * half_rows], wgu[j, n, g * piece : (g + 1) * piece])
+            at = pl.ds(pl.multiple_of(((which * 2 + j) * 4 + n) * half_rows, half_rows), half_rows)
             if g == 0:
-                gu[which, j, n] = part
+                gu[at] = part
             else:
-                gu[which, j, n] = gu[which, j, n] + part
+                gu[at] = gu[at] + part
             return 0
 
         lax.fori_loop(0, 4, body, 0)
 
     def hidden(which, j):
         for i in range(2):
-            gate = gu[which, j, i * 2]
-            hidb[which, j, i] = (gate / (1.0 + jnp.exp(-gate)) * gu[which, j, i * 2 + 1]).astype(BF16)
-
-    def down(which, p, j, dst):
-        g = p // per_col
-
-        def body(n, _):
-            cols = pl.ds(pl.multiple_of((p % per_col) * part_width + n * TILE, TILE), TILE)
-            wide = pl.ds(pl.multiple_of(p * part_width + n * TILE, TILE), TILE)
-            val = dot(hidb[which, j, 0], wd[j, 0, :, wide]) + dot(hidb[which, j, 1], wd[j, 1, :, wide])
-            dst[g, j * half_rows : (j + 1) * half_rows, cols] = val.astype(BF16)
-            return 0
-
-        lax.fori_loop(0, part_width // TILE, body, 0)
-
-    def at_part(ref, p, rows_at):
-        return ref.at[p // per_col, rows_at, pl.ds((p % per_col) * part_width, part_width)]
+            at = ((which * 2 + j) * 4 + i * 2) * half_rows
+            gate = gu[at : at + half_rows]
+            up = gu[at + half_rows : at + 2 * half_rows]
+            hidb[which, j, i] = (gate / (1.0 + jnp.exp(-gate)) * up).astype(BF16)
+
+    def down(which, p, j):
+        wide = slice(starts[p], starts[p] + widths[p])
+        val = dot(hidb[which, j, 0], wd[j, 0, :, wide]) + dot(hidb[which, j, 1], wd[j, 1, :, wide])
+        if which == 0:
+            own[col_of(p), j, :, cols_of(p)] = val.astype(BF16)
+        else:
+            sendbuf[col_of(p), j * half_rows : (j + 1) * half_rows, cols_of(p)] = val.astype(BF16)
+
+    def at_part(ref, p, which, rows_at):
+        return ref.at[col_of(p), which, rows_at, span_of(p)]
 
     def p_copy(p, j):
-        rows_at = pl.ds(j * half_rows, half_rows)
         return remote(
-            at_part(sendbuf, p, rows_at), at_part(xback, p, rows_at), p_sem.at[0, p, j], p_sem.at[1, p, j], token_side[j]
+            sendbuf.at[col_of(p), pl.ds(j * half_rows, half_rows), span_of(p)],
+            at_part(xback, p, j, pl.ds(0, half_rows)),
+            p_sem.at[0, p, j],
+            p_sem.at[1, p, j],
+            token_side[j],
         )
 
-    def r_copy(p, j, r):
-        rows_at = pl.ds(j * half_rows + r * group, group)
+    def r_copy(p, r):
+        rows_at, both = pl.ds(r * group, group), pl.ds(0, 2)
         return remote(
-            at_part(recv, p, rows_at),
-            at_part(ret, p, rows_at),
+            at_part(own, p, both, rows_at),
+            at_part(ret, p, both, rows_at),
             r_sem.at[0, p],
             r_sem.at[1, p],
             at_peer(-(r // NC), -(r % NC)),
         )
+
+    def r_wait(p, side):
+        wait_bytes(at_part(ret, p, pl.ds(0, 2), pl.ds(0, half_rows - group)), r_sem.at[side, p])
 
     def mixer():
         for copy in mix_copies:
@@ -433,9 +489,9 @@
 
     def rs_at(ref, p, d, s, first, count):
         return ref.at[
-            p // per_col,
+            col_of(p),
             pl.ds((d * ring + s) * tok + first, count),
-            pl.ds((p % per_col) * part_width, part_width),
+            span_of(p),
         ]
 
     def rs_copy(p, d, s):
@@ -448,63 +504,61 @@
             at_z(1 - 2 * d),
         )
 
-    def share(p, zi, first, count, adds, place):
-        g = p // per_col
-
-        def body(n, _):
-            cols = pl.ds(pl.multiple_of((p % per_col) * part_width + n * TILE, TILE), TILE)
-            total = dot(back[zi, first : first + count], ret[g, :, cols])
-            for d, s in adds:
-                at = (d * ring + s) * tok + first
-                total = total + rs_recv[g, at : at + count, cols].astype(F32)
-            if place is None:
-                wide = pl.ds(pl.multiple_of(p * part_width + n * TILE, TILE), TILE)
-                moe_out[first : first + count, wide] = (total + shared[first : first + count, wide]).astype(BF16)
-            else:
-                hbuf[g, place + first : place + first + count, cols] = total.astype(BF16)
-            return 0
-
-        lax.fori_loop(0, part_width // TILE, body, 0)
+    def sums_at(p, zi, first, count):
+        at = (p % (gu.shape[0] // (nz * tok))) * nz * tok + zi * tok + first
+        return slice(at, at + count)
+
+    def sums(p):
+        cols = cols_of(p)
+        came = ret[col_of(p), :, :, cols].reshape(2 * half_rows, widths[p])
+        gu[sums_at(p, 0, 0, nz * tok), : widths[p]] = dot(back[...], came)
+
+    def rs_value(p, zi, first, count, adds):
+        total = gu[sums_at(p, zi, first, count), : widths[p]]
+        cols = cols_of(p)
+        for d, s in adds:
+            at = (d * ring + s) * tok + first
+            total = total + rs_recv[col_of(p), at : at + count, cols].astype(F32)
+        return total
 
     def rs_step(p, s):
+        cols = cols_of(p)
         for d in range(2):
             zi = ring - s if d == 0 else ring + s
             place = (d * ring + s) * tok
             if s > 0:
                 with jax.named_scope(f"rswait{p}_{s}"):
                     rs_copy(p, d, s - 1).wait_recv()
-            if s == 0:
-                share(p, zi, d * half, half, (), place)
-            elif s == 1:
-                for h in range(2):
-                    share(p, zi, h * half, half, ((d, 0),) if h == d else (), place)
-            else:
-                share(p, zi, 0, tok, ((d, s - 1),), place)
+            for h in range(2):
+                if s > 0 or h == d:
+                    adds = ((d, s - 1),) if s > 1 or (s == 1 and h == d) else ()
+                    at = place + h * half
+                    hbuf[col_of(p), at : at + half, cols] = rs_value(p, zi, h * half, half, adds).astype(BF16)
             rs_copy(p, d, s).start()
 
     def rs_last(p):
         with jax.named_scope(f"rswait{p}_last"):
             for d in range(2):
                 rs_copy(p, d, ring - 1).wait_recv()
-        share(p, 0, 0, tok, ((0, ring - 1), (1, ring - 1)), None)
+        wide = slice(starts[p], starts[p] + widths[p])
+        total = rs_value(p, 0, 0, tok, ((0, ring - 1), (1, ring - 1)))
+        moe_out[:, wide] = (total + shared[:, wide]).astype(BF16)
 
     def ret_wait(p):
         with jax.named_scope(f"retwait{p}"):
-            far_rows = 2 * (half_rows - group)
-            wait_bytes(at_part(ret, p, pl.ds(0, far_rows)), r_sem.at[1, p])
+            r_wait(p, 1)
+        sums(p)
 
     def give_back(p):
-        cols = slice((p % per_col) * part_width, (p % per_col + 1) * part_width)
-        g = p // per_col
+        cols = cols_of(p)
+        g = col_of(p)
         for j in range(2):
             with jax.named_scope(f"pwait{p}{j}"):
                 p_copy(p, j).wait_recv()
-            span = slice(j * half_rows, (j + 1) * half_rows)
-            recv[g, span, cols] = (recv[g, span, cols].astype(F32) + xback[g, span, cols].astype(F32)).astype(BF16)
-            for r in order[::-1]:
-                r_copy(p, j, r).start()
-            first = slice(j * half_rows, j * half_rows + group)
-            ret[g, first, cols] = recv[g, first, cols]
+            own[g, j, :, cols] = (own[g, j, :, cols].astype(F32) + xback[g, j, :, cols].astype(F32)).astype(BF16)
+        for r in order[::-1]:
+            r_copy(p, r).start()
+        ret[g, :, 0:group, cols] = own[g, :, 0:group, cols]
 
     for s in range(1, ring):
         with jax.named_scope(f"z0_{s}"):
@@ -515,6 +569,8 @@
             z_forward(0, s)
     z_first(1)
     meta_copy(0, ring - 1).wait_recv()
+    for copy in loads[1:]:
+        copy.wait()
     with jax.named_scope("tables"):
         for zi in range(nz):
             tables(zi)
@@ -528,8 +584,6 @@
             z_forward(1, s)
         with jax.named_scope(f"xfwd0_{s}"):
             x_forward(0, order[(s - 1) * len(order) // ring : s * len(order) // ring])
-        for j in range(2):
-            down_copy(j, s - 1).start()
     with jax.named_scope("xfwd0_rest"):
         x_forward(0, order[(ring - 1) * len(order) // ring :])
     with jax.named_scope("last_z1"):
@@ -537,9 +591,11 @@
     with jax.named_scope("select1"):
         select(1)
         y_start(1)
-    for j in range(2):
-        for p in range(ring - 1, PARTS):
-            down_copy(j, p).start()
+    with jax.named_scope("shared_x"):
+        for a in range(3):
+            shared_x_wait(a, 1)
+            for step in range(1, nz):
+                shared_z(a, step).start()
     with jax.named_scope("weights"):
         for j in range(2):
             for copy in own_copies(j):
@@ -551,74 +607,83 @@
             gate_up(0, 0, j)
     with jax.named_scope("xfwd1"):
         x_forward(1, order)
-    with jax.named_scope("shared_x"):
+    with jax.named_scope("shared_z"):
         for a in range(3):
-            shared_x_wait(a, 1)
+            shared_z_wait(a, 1)
             for d in range(2):
                 shared_y(a, d).start()
-    with jax.named_scope("mixer"):
-        mixer()
-    with jax.named_scope("shared_y"):
-        for a in range(3):
-            for d in range(2):
-                shared_y(a, d).wait_recv()
-            shared_y2(a).start()
-            for dy in (0, 1, -1):
-                shared_core(a, dy).start()
+    for p in range(AHEAD):
+        for j in range(2):
+            down_copy(j, p).start()
+    with jax.named_scope("own_gu1"):
+        for j in range(2):
+            gate_up(0, 1, j)
+            hidden(0, j)
     for j in range(2):
         with jax.named_scope(f"xwait0_{j}"):
             wait_bytes(xrecv.at[0, pl.ds(j * half_rows, half_rows)], x_sem.at[1, 0, j])
         with jax.named_scope("par_gu0"):
             gate_up(1, 0, j)
-    with jax.named_scope("own_gu1"):
-        for j in range(2):
-            gate_up(0, 1, j)
-            hidden(0, j)
+    with jax.named_scope("mixer"):
+        mixer()
     far_rows = 2 * (half_rows - group)
     for g in range(COLS):
         wait_bytes(sendbuf.at[g, pl.ds(0, far_rows)], ys_sem.at[g])
+        for d in range(2):
+            for s in range(ring):
+                for h in range(2):
+                    if sends_half(d, s, h):
+                        z_copy(g, d, s, h).wait_send()
     for j in range(2):
         with jax.named_scope(f"xwait1_{j}"):
             wait_bytes(xrecv.at[1, pl.ds(j * half_rows, half_rows)], x_sem.at[1, 1, j])
         with jax.named_scope("par_gu1"):
             gate_up(1, 1, j)
             hidden(1, j)
-    for p in range(PARTS):
+
+    def downs(p):
         for j in range(2):
             with jax.named_scope(f"wd{p}{j}"):
                 down_copy(j, p).wait_recv()
-            with jax.named_scope("par_down"):
-                down(1, p, j, sendbuf)
-                p_copy(p, j).start()
-    for g in range(COLS):
-        for j in range(2):
-            wait_bytes(recv.at[g, pl.ds(0, half_rows)], x_sem.at[0, g, j])
-    with jax.named_scope("own_down"):
-        for p in range(PARTS):
-            for j in range(2):
-                down(0, p, j, recv)
-    for g in range(COLS):
-        for d in range(2):
-            for s in range(ring):
-                for h in range(2):
-                    if sends_half(d, s, h):
-                        z_copy(g, d, s, h).wait_send()
-    with jax.named_scope("shared"):
-        for a in range(3):
-            shared_y2(a).wait_recv()
-            shared_core(a, 2).start()
-        shared_expert()
-
-    events = []
+            down(1, p, j)
+            p_copy(p, j).start()
+            if p + AHEAD < PARTS:
+                down_copy(j, p + AHEAD).start()
+        for j in range(2):
+            down(0, p, j)
+
+    def shared_step(step):
+        with jax.named_scope(f"shared{step}"):
+            for a in range(3):
+                if step == 0:
+                    for d in range(2):
+                        shared_y(a, d).wait_recv()
+                    shared_y2(a).start()
+                    for dy in (0, 1, -1):
+                        shared_core(a, dy).start()
+                if step == 1:
+                    shared_y2(a).wait_recv()
+                    shared_core(a, 2).start()
+            if step == 2:
+                shared_expert()
+
+    events = [(when, shared_step, (step,)) for step, when in enumerate(SHARED_AT)]
     for p in range(PARTS):
-        events.append((9 * p, give_back, (p,)))
-        events.append((9 * p + 11, ret_wait, (p,)))
+        start = GAP * starts[p] / (256 * scale)
+        full = GAP * widths[p] / (256 * scale)
+        events.append((start - LEAD, downs, (p,)))
+        events.append((start + full + GIVE, give_back, (p,)))
+        come = start + full + GIVE + 3.0 + 6.0 * widths[p] / (256 * scale)
+        events.append((come, ret_wait, (p,)))
         for s in range(ring):
-            events.append((9 * p + 12 + 5 * s, rs_step, (p, s)))
-        events.append((9 * p + 12 + 5 * ring, rs_last, (p,)))
+            events.append((come + 0.1 + HOP * s, rs_step, (p, s)))
+        events.append((max(come + 0.1 + HOP * ring, SHARED_AT[2] + 0.1), rs_last, (p,)))
     for _, act, args in sorted(events, key=lambda e: e[0]):
         act(*args)
 
+    for g in range(COLS):
+        for j in range(2):
+            wait_bytes(recv.at[g, pl.ds(0, half_rows)], x_sem.at[0, g, j])
     pltpu.make_async_copy(mixed, mix_out, mix_sem.at[2]).wait()
     halo_copy.wait_send()
     for d in range(2):
@@ -626,7 +691,7 @@
             if meta_goes(d, s):
                 meta_copy(d, s).wait_send()
     for p in range(PARTS):
-        wait_bytes(at_part(ret, p, pl.ds(0, far_rows)), r_sem.at[0, p])
+        r_wait(p, 0)
         for d in range(2):
             for s in range(ring):
                 rs_copy(p, d, s).wait_send()
@@ -638,6 +703,7 @@
             copy.wait_send()
     for a in range(3):
         shared_x_wait(a, 0)
+        shared_z_wait(a, 0)
         shared_y2(a).wait_send()
         shared_core_wait(a, 0)
         for d in range(2):
@@ -664,22 +730,23 @@
     return pl.pallas_call(
         functools.partial(fused_kernel, dims),
         out_shape=(jax.ShapeDtypeStruct((count, width), BF16), jax.ShapeDtypeStruct((tok, width), BF16)),
-        in_specs=[vmem] * 10 + [hbm] * 8,
+        in_specs=[hbm] + [vmem] * 3 + [hbm] * 4 + [vmem] * 2 + [hbm] * 8,
         out_specs=(hbm, vmem),
         scratch_shapes=[
             pltpu.VMEM((COLS, nz * tok, piece), BF16),
             pltpu.VMEM((nz, 16, tok), BF16),
             pltpu.VMEM((rows, nz * tok), BF16),
-            pltpu.VMEM((nz, tok, rows), BF16),
+            pltpu.VMEM((nz * tok, rows), BF16),
             pltpu.VMEM((2, 4, width, hid), BF16),
             pltpu.VMEM((2, 2, hid, width), BF16),
             pltpu.VMEM((COLS, rows, piece), BF16),
             pltpu.VMEM((COLS, rows, piece), BF16),
             pltpu.VMEM((COLS, rows, piece), BF16),
-            pltpu.VMEM((2, 2, 4, half_rows, hid), F32),
+            pltpu.VMEM((16 * half_rows, hid), F32),
             pltpu.VMEM((2, 2, 2, half_rows, hid), BF16),
-            pltpu.VMEM((COLS, rows, piece), BF16),
-            pltpu.VMEM((COLS, rows, piece), BF16),
+            pltpu.VMEM((COLS, 2, half_rows, piece), BF16),
+            pltpu.VMEM((COLS, 2, half_rows, piece), BF16),
+            pltpu.VMEM((COLS, 2, half_rows, piece), BF16),
             pltpu.VMEM((COLS, nz * tok, piece), BF16),
             pltpu.VMEM((tok, width), F32),
             pltpu.VMEM((nx, width, sh), BF16),
@@ -688,6 +755,11 @@
             pltpu.VMEM((count, width), BF16),
             pltpu.VMEM((16, width), BF16),
             pltpu.VMEM(pool.shape, BF16),
+            pltpu.VMEM((tok, width), BF16),
+            pltpu.VMEM((rows, 2 * peers), BF16),
+            pltpu.VMEM((2 * peers, rows), BF16),
+            pltpu.VMEM((rows, nz), F32),
+            pltpu.VMEM((nz, rows), F32),
             pltpu.VMEM((count, width // len(WINDOWS)), BF16),
             pltpu.VMEM((count, width), BF16),
             dma((2, 2, ring)),
@@ -704,9 +776,11 @@
             dma((2, 3)),
             dma((2, 3, 2)),
             dma((2, 3)),
+            dma((2, 3)),
             dma((3, 3)),
             dma((3,)),
             dma((2,)),
+            dma((5,)),
         ],
         compiler_params=pltpu.CompilerParams(
             collective_id=0, has_side_effects=True, vmem_limit_bytes=67043328
@@ -714,8 +788,8 @@
     )(
         moe_input,
         moe_gain.reshape(1, width),
-        ids,
-        scores,
+        ids.T,
+        scores.T,
         jnp.asarray(rep, BF16),
         jnp.asarray(rep.T, BF16),
         jnp.asarray(tgt),

time: 213 us -> 182 us (0.85)
  Pallas kernels: 204 us -> 178 us
  local copies, waits for them, and re-layouts: 6.12 us -> 3.16 us
    pallas_call x1, Pallas kernels: 204 us -> 178 us  [fused(): pl.pallas_call(functools.partial(fused_kernel, dims), out_shape=(jax.Shap...]
    unnamed x6 -> x4, local copies, waits for them, and re-layouts: 6.12 us -> 3.16 us
where the time goes in v3:
time: 182 us; the launch traced here: 181 us
  Pallas kernels  178 us (98%)
  local copies, waits for them, and re-layouts  3.16 us (2%)
    pallas_call x1, Pallas kernels, fused(): pl.pallas_call(functools.partial(fused_kernel, dims), out_shape=(jax.Shap...  178 us

profile of v3, /device:TPU:32, one launch (start us, length us, event | category | flops | bytes accessed | tf_op | source)
XLA Modules:
  0.0 181.4 jit_solution(4800305971277315476)
XLA Ops:
  0.6 177.5 %shard_map.185 = (bf16[256,2048]{1,0:T(8,128)(2,1)}, bf16[128,2048]{1,0:T(8,128)(2,1)}) custom-call(bf16[128,2048]{1,0:T(8,128)(2,1)} %x_hbm.1, f32[1,2048]{1,0:T(1,128)} %bitcast.5, s32[4,512]{1,0:T(4,128)} %bitcast.6, f32[4,128]{1,0:T(4,128)} %bitcast.9, bf16[768,16]{1,0:T(8,128)(2,1)} %constant.8.clone.rep_hbm, bf16[16,768]{1,0:T(8,128)(2,1)} %constant.9.clone.rept_hbm, ...), custom_call_target="tpu_custom_call" | custom-call | tf_op jit(solution)/shard_map/pallas_call | solution.py:730
  178.2 0.0 copy-start
  178.2 2.4 %copy.22 = bf16[256,2048]{1,0:T(8,128)(2,1)} copy(bf16[256,2048]{1,0:T(8,128)(2,1)} %get-tuple-element.4) | data formatting | bytes 2097152
  180.6 0.0 copy-done
  180.6 0.8 copy.23
Async XLA Ops:
  178.2 2.4 %copy-start = (bf16[128,2048]{1,0:T(8,128)(2,1)S(1)}, bf16[128,2048]{1,0:T(8,128)(2,1)}, u32[]{:S(2)}) copy-start(bf16[128,2048]{1,0:T(8,128)(2,1)} %get-tuple-element.5) | copy-start | bytes 1572868

commit v4 on v3

--- a/solution.py
+++ b/solution.py
@@ -803,6 +803,45 @@
     )
 
 
+def hand_over_kernel(mix_in, moe_in, mix_out, moe_out, mix_buf, moe_buf, in_sem, out_sem):
+    pairs = ((mix_in, mix_buf, mix_out), (moe_in, moe_buf, moe_out))
+    steps = []
+    for src, buf, dst in pairs:
+        for at in range(0, src.shape[0], 64):
+            rows = pl.ds(at, 64)
+            i = len(steps)
+            steps.append(
+                (
+                    pltpu.make_async_copy(src.at[rows], buf.at[rows], in_sem.at[i]),
+                    pltpu.make_async_copy(buf.at[rows], dst.at[rows], out_sem.at[i]),
+                )
+            )
+    for come, _ in steps:
+        come.start()
+    for come, go in steps:
+        come.wait()
+        go.start()
+    for _, go in steps:
+        go.wait()
+
+
+def hand_over(mix, moe):
+    hbm = pl.BlockSpec(memory_space=pl.ANY)
+    count = (mix.shape[0] + moe.shape[0]) // 64
+    return pl.pallas_call(
+        hand_over_kernel,
+        out_shape=(jax.ShapeDtypeStruct(mix.shape, BF16), jax.ShapeDtypeStruct(moe.shape, BF16)),
+        in_specs=[hbm, hbm],
+        out_specs=(hbm, hbm),
+        scratch_shapes=[
+            pltpu.VMEM(mix.shape, BF16),
+            pltpu.VMEM(moe.shape, BF16),
+            pltpu.SemaphoreType.DMA((count,)),
+            pltpu.SemaphoreType.DMA((count,)),
+        ],
+    )(mix, moe)
+
+
 def per_device(
     sizes,
     mix_input,
@@ -825,7 +864,7 @@
     experts = lax.axis_size("ep") * expert_gate.shape[0]
     cap = 3 * tok * expert_ids.shape[1] // (2 * experts)
     dims = (nz, ny, lax.axis_size("tp"), tok, cap, width)
-    return fused(
+    mixed, routed_out = fused(
         dims,
         moe_input,
         moe_gain,
@@ -838,6 +877,7 @@
         (expert_gate, expert_up, expert_down),
         (shared_gate, shared_up, shared_down),
     )
+    return hand_over(mixed, routed_out)
 
 
 def solution(mesh, sizes=(NZ, NY)):

time: 182 us -> 181 us (level)
  local copies, waits for them, and re-layouts: 3.16 us -> 0 us
  Pallas kernels: 178 us -> 180 us
    unnamed x4 -> x0, local copies, waits for them, and re-layouts: 3.16 us -> none
    pallas_call x0 -> x1, Pallas kernels: none -> 2.19 us  [hand_over(): pl.pallas_call(hand_over_kernel, out_shape=(jax.ShapeDtypeStruct(mix.shap...]
where the time goes in v4:
time: 181 us
  Pallas kernels  180 us (99%)
    pallas_call x1, Pallas kernels, fused(): pl.pallas_call(functools.partial(fused_kernel, dims), out_shape=(jax.Shap...  178 us

profile of v4, /device:TPU:32, one launch (start us, length us, event | category | flops | bytes accessed | tf_op | source)
XLA Modules:
  0.0 180.6 jit_solution(58702234631544743)
XLA Ops:
  0.6 177.5 %shard_map.185 = (bf16[256,2048]{1,0:T(8,128)(2,1)}, bf16[128,2048]{1,0:T(8,128)(2,1)}) custom-call(bf16[128,2048]{1,0:T(8,128)(2,1)} %x_hbm.1, f32[1,2048]{1,0:T(1,128)} %bitcast.5, s32[4,512]{1,0:T(4,128)} %bitcast.6, f32[4,128]{1,0:T(4,128)} %bitcast.9, bf16[768,16]{1,0:T(8,128)(2,1)} %constant.8.clone.rep_hbm, bf16[16,768]{1,0:T(8,128)(2,1)} %constant.9.clone.rept_hbm, ...), custom_call_target="tpu_custom_call" | custom-call | tf_op jit(solution)/shard_map/pallas_call | solution.py:730
  178.2 2.2 %shard_map.186 = (bf16[256,2048]{1,0:T(8,128)(2,1)}, bf16[128,2048]{1,0:T(8,128)(2,1)}) custom-call(bf16[256,2048]{1,0:T(8,128)(2,1)} %get-tuple-element.4.mix_in, bf16[128,2048]{1,0:T(8,128)(2,1)} %get-tuple-element.5.moe_in), custom_call_target="tpu_custom_call" | custom-call | tf_op jit(solution)/shard_map/pallas_call | solution.py:831
